TPU v7x, 768 devices: a whole 4x8x12 slice. The times are simulated.
768 devices in a mesh: ep: 48 (over z, x), tp: 16 (over y, core).
Axes of the slice: x: 4, y: 8, z: 12, core: 2. Of those that a mesh axis runs over, the one named last changes fastest.
Arguments:
- tokens: bfloat16 [1152, 2048], P('ep'), may hold values from -12 to 12
- state: float32 [1152, 16, 128, 256], P('ep', 'tp'), may hold values from -6 to 6
- w_query: bfloat16 [2048, 2048], P(None, 'tp'), may hold values from -0.125 to 0.125
- w_key: bfloat16 [2048, 2048], P(None, 'tp'), may hold values from -0.125 to 0.125
- w_value: bfloat16 [2048, 4096], P(None, 'tp'), may hold values from -0.125 to 0.125
- w_outgate: bfloat16 [2048, 4096], P(None, 'tp'), may hold values from -0.125 to 0.125
- decay_down: bfloat16 [2048, 16], replicated, may hold values from -0.125 to 0.125
- decay_up: bfloat16 [16, 2048], P(None, 'tp'), may hold values from -9 to 9
- decay_bias: float32 [2048], P('tp'), may hold values from -6 to 4
- head_gain: float32 [256], replicated, may hold values from 0.1 to 1.9
- w_output: bfloat16 [4096, 2048], P('tp'), may hold values from -0.09375 to 0.09375
- norm1_gain: float32 [2048], P('tp'), may hold values from 0.1 to 1.9
- route_ids: int32 [1152, 6], P('ep'), may hold values from 0 to 191, all different within a row; in each aligned block of 24 rows (0 to 23, 24 to 47, ...) at most 2 rows name the same one
- route_weight: float32 [1152, 6], P('ep'), may hold values from 0.1 to 1
- exp_gate: bfloat16 [192, 2048, 512], P('ep', 'tp'), may hold values from -0.125 to 0.125
- exp_up: bfloat16 [192, 2048, 512], P('ep', 'tp'), may hold values from -0.125 to 0.125
- exp_down: bfloat16 [192, 512, 2048], P('ep', None, 'tp'), may hold values from -0.25 to 0.25
- sh_gate: bfloat16 [2048, 512], P('tp'), may hold values from -0.125 to 0.125
- sh_up: bfloat16 [2048, 512], P('tp'), may hold values from -0.125 to 0.125
- sh_down: bfloat16 [512, 2048], P(None, 'tp'), may hold values from -0.25 to 0.25
- norm2_gain: float32 [2048], P('tp'), may hold values from 0.1 to 1.9
Outputs:
- layer_out: bfloat16 [1152, 2048], P('ep', 'tp')
Inputs may be any that keep to these rules, and one draw needn't show every extreme that they name: `route_ids`: each row names 6 different experts. Among the rows of one index of ep (aligned blocks of 24 rows) no expert is named by more than 2 rows, and in some blocks one expert is named by exactly 2.
All inputs are finite; a program needn't handle non-finite values.
Results may differ from a plain program's by a relative error of at most 0.02.
Values may be sent and summed in bfloat16 or wider, within the bound.
No kernel may reach another device: no remote copies, remote signals or barrier semaphores. Data moves between devices by JAX's collectives and lax.ppermute only.
A program may use at most 32 MiB of HBM per device.

v0:
```python
import jax
import jax.numpy as jnp
from jax import lax
from jax.sharding import PartitionSpec as P

res_scale = 2.0**0.5
decay_tau = 16.0
norm_eps = 1e-05


def split_up(value, dim, size):
    before, after = (value.shape[:dim], value.shape[dim + 1 :])
    return jnp.moveaxis(value.reshape(*before, size, -1, *after), dim, 0)


def sum_at_owner(value, axis, dim):
    tiles = split_up(value, dim, lax.axis_size(axis))
    arrived = lax.all_to_all(tiles, axis, split_axis=0, concat_axis=0, tiled=True)
    return arrived.astype(jnp.float32).sum(axis=0)


def copy_for_each(value, axis):
    size = lax.axis_size(axis)
    return lax.all_to_all(
        jnp.broadcast_to(value[None], (size, *value.shape)), axis, 0, 0, tiled=True
    )


def over_copies(value, axis):
    return copy_for_each(value, axis).sum(axis=0)


def in_one(arrays, axis):
    ends = [0]
    for a in arrays:
        ends.append(ends[-1] + a.size)
    so_far = over_copies(jnp.concatenate([a.ravel() for a in arrays]), axis)
    return tuple((so_far[b:e].reshape(a.shape) for a, b, e in zip(arrays, ends, ends[1:])))


def one_scatter(arrays, axis, dims):
    size = lax.axis_size(axis)
    tiles = [split_up(a, dim, size) for a, dim in zip(arrays, dims)]
    lines = jnp.concatenate([b.reshape(size, -1) for b in tiles], axis=1)
    rows = max(16, -(-lines.shape[1] // 1024) * 8)
    lines = jnp.pad(lines, ((0, 0), (0, rows * 128 - lines.shape[1]))).reshape(-1, 128)
    flat, at, gathered = (lax.psum_scatter(lines, axis, tiled=True).reshape(-1), 0, [])
    for b in tiles:
        part = b[0]
        gathered.append(flat[at : at + part.size].reshape(part.shape))
        at += part.size
    return tuple(gathered)


def rows_first(arrays, axis, dims):
    turned = [jnp.moveaxis(a, dim, 0) for a, dim in zip(arrays, dims)]
    widths = [t[0].size for t in turned]
    both = jnp.concatenate([t.reshape(-1, w) for t, w in zip(turned, widths)], axis=1)
    filled = lax.all_gather(both, axis, axis=0, tiled=True)
    tiles = jnp.split(filled, [sum(widths[:k]) for k in range(1, len(widths))], axis=1)
    return tuple(
        (
            jnp.moveaxis(b.reshape(-1, *t.shape[1:]), 0, dim)
            for b, t, dim in zip(tiles, turned, dims)
        )
    )


def settle(values):
    return lax.optimization_barrier(values.astype(jnp.bfloat16)).astype(jnp.float32)


def project(left, right):
    return jnp.dot(left, right, preferred_element_type=jnp.float32)


def apply_norm(values, sums, squares, width, gain):
    mean_val = sums[:, None] / width
    spread = squares[:, None] / width - mean_val * mean_val
    return (values - mean_val) * lax.rsqrt(spread + norm_eps) * gain


def per_device(
    tokens,
    state,
    w_query,
    w_key,
    w_value,
    w_outgate,
    decay_down,
    decay_up,
    decay_bias,
    head_gain,
    w_output,
    norm1_gain,
    route_ids,
    route_weight,
    exp_gate,
    exp_up,
    exp_down,
    sh_gate,
    sh_up,
    sh_down,
    norm2_gain,
):
    row_count, width = tokens.shape
    head_count, key_dim, val_dim = (state.shape[1], state.shape[2], state.shape[3])
    tp_count = lax.axis_size("tp")
    ep_count = lax.axis_size("ep")
    col_count = width // tp_count
    col_start = lax.axis_index("tp") * col_count
    queries = settle(project(tokens, w_query)).reshape(
        row_count, head_count, key_dim
    ) * key_dim ** (-0.5)
    key_rows = settle(project(tokens, w_key)).reshape(row_count, head_count, key_dim)
    values = settle(project(tokens, w_value)).reshape(row_count, head_count, val_dim)
    gate_pre = settle(project(tokens, w_outgate)).reshape(row_count, head_count, val_dim)
    decay_low = lax.optimization_barrier(project(tokens, decay_down).astype(jnp.bfloat16))
    log_decay = (jax.nn.log_sigmoid(project(decay_low, decay_up) + decay_bias) / decay_tau).reshape(
        row_count, head_count, key_dim
    )
    carried = jnp.einsum(
        "bhk,bhkv->bhv", queries * jnp.exp(log_decay), state, precision=lax.Precision.HIGHEST
    )
    attended = carried + jnp.sum(queries * key_rows, -1, keepdims=True) * values
    inv_norm = lax.rsqrt(jnp.mean(attended * attended, -1, keepdims=True) + norm_eps)
    head_out = (
        (attended * inv_norm * head_gain * jax.nn.silu(gate_pre))
        .astype(jnp.bfloat16)
        .reshape(row_count, head_count * val_dim)
    )
    partial_out = project(head_out, w_output)
    mixed = settle(sum_at_owner(partial_out.astype(jnp.bfloat16), "tp", 1))
    own_tokens = lax.dynamic_slice_in_dim(tokens, col_start, col_count, 1).astype(jnp.float32)
    own_resid = res_scale * own_tokens + mixed
    first_sums, first_squares = in_one(
        (jnp.sum(own_resid, -1), jnp.sum(own_resid * own_resid, -1)), "tp"
    )
    normed_mid = apply_norm(own_resid, first_sums, first_squares, width, norm1_gain)
    normed_mid = lax.optimization_barrier(normed_mid.astype(jnp.bfloat16))
    top_count = route_ids.shape[1]
    local_count = exp_gate.shape[0]
    expert_count = local_count * ep_count
    capacity = max(2, row_count * top_count // expert_count + 1)
    flat_ids = route_ids.reshape(row_count * top_count)
    onehot = (flat_ids[:, None] == jnp.arange(expert_count, dtype=jnp.int32)[None, :]).astype(
        jnp.int32
    )
    ranks = jnp.sum((jnp.cumsum(onehot, 0) - 1) * onehot, 1)
    slots = flat_ids * capacity + ranks
    placement = (
        slots[:, None] == jnp.arange(expert_count * capacity, dtype=jnp.int32)[None, :]
    ).astype(jnp.bfloat16)
    pair_rows = jnp.repeat(normed_mid, top_count, axis=0)
    outgoing = jnp.einsum(
        "ps,pc->sc", placement, pair_rows, preferred_element_type=jnp.float32
    ).astype(jnp.bfloat16)
    outgoing = outgoing.reshape(ep_count, local_count, capacity, col_count)
    incoming = lax.all_to_all(outgoing, "ep", split_axis=0, concat_axis=0, tiled=True)
    gate_part = jnp.einsum("secd,edf->secf", incoming, exp_gate, preferred_element_type=jnp.float32)
    up_part = jnp.einsum("secd,edf->secf", incoming, exp_up, preferred_element_type=jnp.float32)
    shared_gate_part = project(normed_mid, sh_gate)
    shared_up_part = project(normed_mid, sh_up)
    gate_sum, up_sum, shared_gate_sum, shared_up_sum = tuple(
        (
            part.astype(jnp.float32)
            for part in one_scatter(
                (
                    gate_part.astype(jnp.bfloat16),
                    up_part.astype(jnp.bfloat16),
                    shared_gate_part.astype(jnp.bfloat16),
                    shared_up_part.astype(jnp.bfloat16),
                ),
                "tp",
                (3, 3, 1, 1),
            )
        )
    )
    inner_share = (jax.nn.silu(settle(gate_sum)) * settle(up_sum)).astype(jnp.bfloat16)
    shared_share = (jax.nn.silu(settle(shared_gate_sum)) * settle(shared_up_sum)).astype(
        jnp.bfloat16
    )
    inner, shared_inner = rows_first((inner_share, shared_share), "tp", (3, 1))
    expert_out = jnp.einsum(
        "secf,efd->secd", inner, exp_down, preferred_element_type=jnp.float32
    ).astype(jnp.bfloat16)
    returned = lax.all_to_all(expert_out, "ep", split_axis=0, concat_axis=0, tiled=True)
    picked = jnp.einsum(
        "ps,sc->pc",
        placement,
        returned.reshape(expert_count * capacity, col_count),
        preferred_element_type=jnp.float32,
    )
    routed = jnp.sum(picked.reshape(row_count, top_count, col_count) * route_weight[:, :, None], 1)
    mixture = routed + project(shared_inner, sh_down)
    out_resid = res_scale * normed_mid.astype(jnp.float32) + mixture
    last_sums, last_squares = in_one(
        (jnp.sum(out_resid, -1), jnp.sum(out_resid * out_resid, -1)), "tp"
    )
    return apply_norm(out_resid, last_sums, last_squares, width, norm2_gain).astype(jnp.bfloat16)


def solution(mesh):
    in_specs = (
        P("ep", None),
        P("ep", "tp", None, None),
        P(None, "tp"),
        P(None, "tp"),
        P(None, "tp"),
        P(None, "tp"),
        P(),
        P(None, "tp"),
        P("tp"),
        P(),
        P("tp", None),
        P("tp"),
        P("ep", None),
        P("ep", None),
        P("ep", "tp", None),
        P("ep", "tp", None),
        P("ep", None, "tp"),
        P("tp", None),
        P("tp", None),
        P(None, "tp"),
        P("tp"),
    )
    out_specs = P("ep", "tp")
    return jax.shard_map(
        per_device, mesh=mesh, in_specs=in_specs, out_specs=out_specs, check_vma=False
    )
```

profile of v0, /device:TPU:1, one launch (start us, length us, event | category | flops | bytes accessed | tf_op | source)
XLA Modules:
  0.0 232.7 jit_solution(13759181623354748670)
XLA Ops:
  6.5 1.4 convolution_convert_fusion.10
  8.0 1.1 convolution_convert_fusion.11
  9.0 1.3 convolution_convert_fusion.9
  10.3 1.5 convolution_convert_fusion.8
  12.3 1.6 fusion
  15.3 14.4 %all-to-all-start = ((bf16[16,24,128]{2,1,0:T(8,128)(2,1)}), bf16[16,24,128]{2,1,0:T(8,128)(2,1)}, u32[]{:S(2)}, u32[]{:S(2)}) async-start(bf16[16,24,128]{2,1,0:T(8,128)(2,1)} %bitcast.105), calls=%async_computation | async-start | bytes 196608 | tf_op jit(solution)/shard_map/all_to_all | solution.py:18
  32.5 1.1 fusion.61
  34.3 1.1 copy.127
  37.1 1.2 all-to-all-done
  40.0 6.1 %all-to-all-start.1 = ((f32[16,1,48]{2,1,0:T(1,128)}), f32[16,1,48]{2,1,0:T(1,128)S(1)}, u32[]{:S(2)}, u32[]{:S(2)}) async-start(f32[16,1,48]{2,1,0:T(1,128)} %broadcast_in_dim.6), calls=%async_computation.1 | async-start | bytes 16384 | tf_op jit(solution)/shard_map/all_to_all | solution.py:24
  46.1 7.0 %all-to-all-done.1 = f32[16,1,48]{2,1,0:T(1,128)S(1)} async-done(((f32[16,1,48]{2,1,0:T(1,128)}), f32[16,1,48]{2,1,0:T(1,128)S(1)}, u32[]{:S(2)}, u32[]{:S(2)}) %all-to-all-start.1) | async-done | bytes 3104 | tf_op jit(solution)/shard_map/all_to_all | solution.py:24
  54.4 12.4 %all-to-all-start.2 = ((bf16[48,4,2,128]{3,2,1,0:T(2,128)(2,1)}), bf16[48,4,2,128]{3,2,1,0:T(2,128)(2,1)}, u32[]{:S(2)}, u32[]{:S(2)}) async-start(bf16[48,4,2,128]{3,2,1,0:T(2,128)(2,1)} %bitcast.9), calls=%async_computation.2 | async-start | bytes 196608 | tf_op jit(solution)/shard_map/all_to_all | solution.py:159
  70.9 7.2 %all-to-all-done.2 = bf16[48,4,2,128]{3,2,1,0:T(2,128)(2,1)} async-done(((bf16[48,4,2,128]{3,2,1,0:T(2,128)(2,1)}), bf16[48,4,2,128]{3,2,1,0:T(2,128)(2,1)}, u32[]{:S(2)}, u32[]{:S(2)}) %all-to-all-start.2) | async-done | bytes 98336 | tf_op jit(solution)/shard_map/all_to_all | solution.py:159
  78.1 1.4 fusion.6
  79.5 2.0 reshape.200
  81.5 4.2 %copy.130 = bf16[16,48,4,2,32]{4,3,2,1,0:T(2,128)(2,1)} copy(bf16[16,48,4,2,32]{4,0,1,3,2:T(8,128)(2,1)} %bitcast.111) | data formatting | bytes 786432 | tf_op jit(solution)/shard_map/transpose | solution.py:13
  85.7 3.1 %reshape.201 = bf16[16,12288]{1,0:T(8,128)(2,1)S(1)} reshape(bf16[16,48,4,2,32]{4,3,2,1,0:T(2,128)(2,1)} %copy.130) | data formatting | bytes 786432 | tf_op jit(solution)/shard_map/reshape | solution.py:44
  88.7 2.1 fusion.7
  90.8 2.9 %reshape.202 = bf16[48,4,2,16,32]{4,3,0,2,1:T(8,128)(2,1)} reshape(bf16[48,4,2,512]{3,0,2,1:T(8,128)(2,1)} %fusion.7) | data formatting | bytes 786432 | tf_op jit(solution)/shard_map/reshape | solution.py:13
  93.7 4.2 %copy.132 = bf16[16,48,4,2,32]{4,3,2,1,0:T(2,128)(2,1)} copy(bf16[16,48,4,2,32]{4,0,1,3,2:T(8,128)(2,1)} %bitcast.112) | data formatting | bytes 786432 | tf_op jit(solution)/shard_map/transpose | solution.py:13
  97.9 3.8 %reshape.203 = bf16[16,12288]{1,0:T(8,128)(2,1)} reshape(bf16[16,48,4,2,32]{4,3,2,1,0:T(2,128)(2,1)} %copy.132) | data formatting | bytes 786432 | tf_op jit(solution)/shard_map/reshape | solution.py:44
  101.7 2.0 fusion.15
  103.7 2.5 %reshape.208 = bf16[3328,128]{1,0:T(8,128)(2,1)} reshape(bf16[16,26624]{1,0:T(8,128)(2,1)} %fusion.15) | data formatting | bytes 1703936 | tf_op jit(solution)/shard_map/reshape | solution.py:46
  106.2 51.9 %reduce-scatter.2.cloned.1.call-done = bf16[208,128]{1,0:T(8,128)(2,1)} async-done(((bf16[3328,128]{1,0:T(8,128)(2,1)}), bf16[208,128]{1,0:T(8,128)(2,1)}) %reduce-scatter.2.cloned.1.call-update) | async-done | bytes 53264 | tf_op jit(solution)/shard_map/reduce_scatter | solution.py:47
  160.7 17.0 %all_gather.3 = bf16[512,408]{1,0:T(8,128)(2,1)S(1)} all-gather(bf16[32,408]{1,0:T(8,128)(2,1)S(1)} %pad_maximum_fusion), channel_id=1, replica_groups=mesh['ep'=48,'tp'=16] {'tp'}, dimensions={0}, use_global_device_ids=true | all-gather | bytes 443904 | tf_op jit(solution)/shard_map/all_gather | solution.py:59
  179.3 1.2 copy.140
  181.4 1.5 fusion.8
  183.6 13.0 %all-to-all-start.3 = ((bf16[48,4,2,128]{3,2,1,0:T(2,128)(2,1)}), bf16[48,4,2,128]{3,2,1,0:T(2,128)(2,1)S(1)}, u32[]{:S(2)}, u32[]{:S(2)}) async-start(bf16[48,4,2,128]{3,2,1,0:T(2,128)(2,1)} %copy.142), calls=%async_computation.4 | async-start | bytes 196608 | tf_op jit(solution)/shard_map/all_to_all | solution.py:187
  196.8 11.2 %all-to-all-done.3 = bf16[48,4,2,128]{3,2,1,0:T(2,128)(2,1)S(1)} async-done(((bf16[48,4,2,128]{3,2,1,0:T(2,128)(2,1)}), bf16[48,4,2,128]{3,2,1,0:T(2,128)(2,1)S(1)}, u32[]{:S(2)}, u32[]{:S(2)}) %all-to-all-start.3) | async-done | bytes 98336 | tf_op jit(solution)/shard_map/all_to_all | solution.py:187
  209.0 1.3 fusion.58
  210.3 14.1 %all_to_all.27 = f32[16,1,48]{2,1,0:T(1,128)S(1)} all-to-all(f32[16,1,48]{2,1,0:T(1,128)S(1)} %broadcast_in_dim.8), channel_id=1, replica_groups=mesh['ep'=48,'tp'=16] {'tp'}, dimensions={0} | all-to-all | bytes 6144 | tf_op jit(solution)/shard_map/all_to_all | solution.py:24
  224.5 1.3 multiply_convert_fusion
  (86 shorter events, 20.9 us)
Async XLA Ops:
  6.5 5.7 %copy-start = (f32[24,1,128,256]{3,2,1,0:T(8,128)S(1)}, f32[24,1,128,256]{3,2,1,0:T(8,128)}, u32[]{:S(2)}) copy-start(f32[24,1,128,256]{3,2,1,0:T(8,128)} %param.22) | copy-start | bytes 9437188
  6.5 5.5 %copy-start.8 = (bf16[16,128]{1,0:T(8,128)(2,1)S(1)}, bf16[16,128]{1,0:T(8,128)(2,1)}, u32[]{:S(2)}) copy-start(bf16[16,128]{1,0:T(8,128)(2,1)} %param.28) | copy-start | bytes 12292
  6.5 5.5 %copy-start.9 = (f32[128]{0:T(128)S(1)}, f32[128]{0:T(128)}, u32[]{:S(2)}) copy-start(f32[128]{0:T(128)} %param.29) | copy-start | bytes 1540
  11.9 2.2 copy-start.1
  11.9 2.2 copy-start.4
  12.2 2.1 copy-start.3
  12.2 2.1 copy-start.6
  13.9 15.8 %copy-start.5 = (s32[24,6]{0,1:T(8,128)S(1)}, s32[24,6]{0,1:T(8,128)}, u32[]{:S(2)}) copy-start(s32[24,6]{0,1:T(8,128)} %param.33) | copy-start | bytes 1732
  15.3 23.0 %all-to-all-start = ((bf16[16,24,128]{2,1,0:T(8,128)(2,1)}), bf16[16,24,128]{2,1,0:T(8,128)(2,1)}, u32[]{:S(2)}, u32[]{:S(2)}) async-start(bf16[16,24,128]{2,1,0:T(8,128)(2,1)} %bitcast.105), calls=%async_computation | async-start | bytes 196608 | tf_op jit(solution)/shard_map/all_to_all | solution.py:18
  29.9 23.3 %copy-start.7 = (f32[128]{0:T(128)S(1)}, f32[128]{0:T(128)}, u32[]{:S(2)}) copy-start(f32[128]{0:T(128)} %param.32) | copy-start | bytes 1540
  40.0 13.2 %all-to-all-start.1 = ((f32[16,1,48]{2,1,0:T(1,128)}), f32[16,1,48]{2,1,0:T(1,128)S(1)}, u32[]{:S(2)}, u32[]{:S(2)}) async-start(f32[16,1,48]{2,1,0:T(1,128)} %broadcast_in_dim.6), calls=%async_computation.1 | async-start | bytes 16384 | tf_op jit(solution)/shard_map/all_to_all | solution.py:24
  54.4 23.7 %all-to-all-start.2 = ((bf16[48,4,2,128]{3,2,1,0:T(2,128)(2,1)}), bf16[48,4,2,128]{3,2,1,0:T(2,128)(2,1)}, u32[]{:S(2)}, u32[]{:S(2)}) async-start(bf16[48,4,2,128]{3,2,1,0:T(2,128)(2,1)} %bitcast.9), calls=%async_computation.2 | async-start | bytes 196608 | tf_op jit(solution)/shard_map/all_to_all | solution.py:159
  66.8 91.4 %reduce-scatter.2.cloned.1.call-start = ((), (), s32[]{:S(2)}) async-start(), calls=%async_computation.6 | async-start | bytes 905216 | tf_op jit(solution)/shard_map/reduce_scatter | solution.py:47
  177.7 0.8 copy-start.2
  183.6 24.4 %all-to-all-start.3 = ((bf16[48,4,2,128]{3,2,1,0:T(2,128)(2,1)}), bf16[48,4,2,128]{3,2,1,0:T(2,128)(2,1)S(1)}, u32[]{:S(2)}, u32[]{:S(2)}) async-start(bf16[48,4,2,128]{3,2,1,0:T(2,128)(2,1)} %copy.142), calls=%async_computation.4 | async-start | bytes 196608 | tf_op jit(solution)/shard_map/all_to_all | solution.py:187
Sparse Core Ops, SparseCore 0:
  106.3 51.7 reduce-scatter.1
where the time goes:
time: 234 us; the launch traced here: 233 us
  waiting for transfers between devices  78.6 us (34%)
  starting transfers between devices  46.1 us (20%)
  local copies, waits for them, and re-layouts  36.5 us (16%)
  blocking collectives  31.1 us (13%)
  matrix products  17.8 us (8%)
  between operations  13.7 us (6%)
  other arithmetic  8.71 us (4%)
    reduce_scatter x1, waiting for transfers between devices, one_scatter(): lax.psum_scatter(lines, axis, tiled=True).reshape(-1)  51.9 us
    all_gather x1, blocking collectives, rows_first(): filled = lax.all_gather(both, axis, axis=0, tiled=True)  17 us
    all_to_all x1, starting transfers between devices, sum_at_owner(): lax.all_to_all(tiles, axis, split_axis=0, concat_axis=0, tiled=True)  14.4 us
    all_to_all x1, blocking collectives, copy_for_each(): lax.all_to_all(jnp.broadcast_to(value[None], (size, *value.shape)), axis,...  14.1 us
    all_to_all x1, starting transfers between devices, per_device(): lax.all_to_all(expert_out, 'ep', split_axis=0, concat_axis=0, tiled=True)  13 us
    all_to_all x1, starting transfers between devices, per_device(): lax.all_to_all(outgoing, 'ep', split_axis=0, concat_axis=0, tiled=True)  12.4 us
    all_to_all x1, waiting for transfers between devices, per_device(): lax.all_to_all(expert_out, 'ep', split_axis=0, concat_axis=0, tiled=True)  11.2 us
    dot_general x10, matrix products, project(): return jnp.dot(left, right, preferred_element_type=jnp.float32)  9.38 us
  transfers between devices with their start and end apart: 5, of which 5 were waited for; matrix products, arithmetic and copies ran while one was open for 5% of the time, Pallas kernels for 0%

commit v1 on v0

v1 whole, which is shorter than its diff:
```python
import jax
import jax.numpy as jnp
from jax import lax
from jax.experimental import pallas as pl
from jax.experimental.pallas import tpu as pltpu
from jax.sharding import PartitionSpec as P

res_scale = 2.0**0.5
decay_tau = 16.0
norm_eps = 1e-05
capacity = 2
lanes = 128

f32 = jnp.float32
bf16 = jnp.bfloat16


def local_call(body, outs, args, unread=0):
    vmem = pl.BlockSpec(memory_space=pltpu.VMEM)
    anywhere = pl.BlockSpec(memory_space=pl.ANY)
    return pl.pallas_call(
        body,
        out_shape=outs,
        in_specs=[vmem] * (len(args) - unread) + [anywhere] * unread,
        out_specs=jax.tree.map(lambda _: vmem, outs),
        name=body.__name__,
    )(*args)


def struct(shape, dtype):
    return jax.ShapeDtypeStruct(shape, dtype)


def iota(shape, dim):
    return lax.broadcasted_iota(jnp.int32, shape, dim)


def dot(left, right):
    return jnp.dot(left, right, preferred_element_type=f32)


def rounded(value):
    return value.astype(bf16).astype(f32)


def as_row(column):
    rows = column.shape[0]
    seen = jnp.where(iota((rows, lanes), 0) == iota((rows, lanes), 1), column, 0.0)
    return jnp.sum(seen, axis=0, keepdims=True)


def as_column(row, rows):
    seen = jnp.where(iota((rows, lanes), 0) == iota((rows, lanes), 1), row, 0.0)
    return jnp.sum(seen, axis=1, keepdims=True)


def silu(value):
    return value * jax.nn.sigmoid(value)


def attend(
    tok_ref, state_ref, wq_ref, wk_ref, wv_ref, wg_ref, dd_ref, du_ref, db_ref, hg_ref, wo_ref, out_ref
):
    rows = tok_ref.shape[0]
    key_dim = wq_ref.shape[1]
    tok = tok_ref[...]
    queries = rounded(dot(tok, wq_ref[...])) * key_dim ** (-0.5)
    keys = rounded(dot(tok, wk_ref[...]))
    values = rounded(dot(tok, wv_ref[...]))
    gate = rounded(dot(tok, wg_ref[...]))
    low = dot(tok, dd_ref[...]).astype(bf16)
    pre = dot(low, du_ref[...]) + db_ref[...]
    log_decay = (jnp.minimum(pre, 0.0) - jnp.log1p(jnp.exp(-jnp.abs(pre)))) / decay_tau
    decayed = queries * jnp.exp(log_decay)
    turned = jnp.concatenate([decayed, jnp.zeros((lanes - rows, key_dim), f32)], axis=0).T
    carried = jnp.concatenate(
        [
            jnp.sum(turned[:, b : b + 1] * state_ref[b, 0], axis=0, keepdims=True)
            for b in range(rows)
        ],
        axis=0,
    )
    attended = carried + jnp.sum(queries * keys, axis=1, keepdims=True) * values
    inv_norm = lax.rsqrt(jnp.mean(attended * attended, axis=1, keepdims=True) + norm_eps)
    head_out = (attended * inv_norm * hg_ref[...] * silu(gate)).astype(bf16)
    partial = rounded(dot(head_out, wo_ref[...]))
    row = as_row(jnp.sum(partial, axis=1, keepdims=True))
    high = rounded(row)
    middle = rounded(row - high)
    low = row - high - middle
    at = iota((8, lanes), 0)
    tail = jnp.where(at == 0, high, jnp.where(at == 1, middle, jnp.where(at == 2, low, 0.0)))
    for j in range(out_ref.shape[0]):
        out_ref[j] = jnp.concatenate(
            [partial[:, j * lanes : (j + 1) * lanes], tail], axis=0
        ).astype(bf16)


def place(ids_ref, turned_ref, weight_ref, behind, send_ref, high_ref, low_ref, perm_ref, back_ref):
    rows, top = ids_ref.shape
    slots = send_ref.shape[0]
    blocks = slots // (4 * capacity)
    slot = iota((slots, lanes), 0)
    hit = jnp.zeros((slots, lanes), f32)
    for k in range(top):
        hit = jnp.where(turned_ref[k : k + 1, :] == slot // capacity, 1.0, hit)
    earlier = (iota((lanes, lanes), 0) < iota((lanes, lanes), 1)).astype(bf16)
    rank = dot(hit.astype(bf16), earlier)
    send_ref[...] = jnp.where(rank == (slot % capacity).astype(f32), hit, 0.0).astype(bf16)
    slot = iota((rows, slots), 1)
    hit = jnp.zeros((rows, slots), f32)
    weight = jnp.zeros((rows, slots), f32)
    for k in range(top):
        same = ids_ref[:, k : k + 1] == slot // capacity
        hit = jnp.where(same, 1.0, hit)
        weight = jnp.where(same, weight_ref[:, k : k + 1], weight)
    earlier = (iota((rows, rows), 1) < iota((rows, rows), 0)).astype(bf16)
    rank = dot(earlier, hit.astype(bf16))
    weight = jnp.where(rank == (slot % capacity).astype(f32), weight, 0.0)
    high = weight.astype(bf16)
    high_ref[...] = high
    low_ref[...] = (weight - high.astype(f32)).astype(bf16)
    per_expert = blocks * capacity

    def source(at):
        expert, rest = at // per_expert, at % per_expert
        return rest // capacity * (4 * capacity) + expert * capacity + rest % capacity

    one, two = iota((slots, slots), 0), iota((slots, slots), 1)
    perm_ref[...] = (source(one) == two).astype(bf16)
    back_ref[...] = (one == source(two)).astype(bf16)


def dispatch(got_ref, tok_ref, own_ref, gain_ref, send_ref, rows_ref, centred_ref):
    rows, width = tok_ref.shape
    total = jnp.sum(got_ref[...].astype(f32), axis=0)
    mixed = rounded(total[:rows])
    sums = total[rows : rows + 1] + total[rows + 1 : rows + 2] + total[rows + 2 : rows + 3]
    tok_sum = jnp.sum(tok_ref[...].astype(f32), axis=1, keepdims=True)
    mean = (res_scale * tok_sum + as_column(sums, rows)) / width
    centred = res_scale * own_ref[...].astype(f32) + mixed - mean
    centred_ref[...] = centred
    scaled = centred * gain_ref[...]
    filled = jnp.concatenate([scaled, jnp.zeros((lanes - rows, lanes), f32)], axis=0)
    rows_ref[...] = dot(send_ref[...], filled.astype(bf16)).astype(bf16)


def two_parts(column):
    high = rounded(column)
    return high, column - high


def expand(rows_ref, perm_ref, gate_ref, up_ref, sg_ref, su_ref, gain_ref, centred_ref, out_ref):
    chunks, rows, width = out_ref.shape
    experts, _, hidden = gate_ref.shape
    sorted_rows = dot(perm_ref[...], rows_ref[...])
    scale = sorted_rows / gain_ref[...]
    high, low = two_parts(jnp.sum(scale * scale, axis=1, keepdims=True))
    centred = centred_ref[...]
    own_high, own_low = two_parts(jnp.sum(centred * centred, axis=1, keepdims=True))
    own = (centred * gain_ref[...]).astype(bf16)
    shared_gate, shared_up = dot(own, sg_ref[...]), dot(own, su_ref[...])
    lane = iota((rows, lanes), 1)
    share = hidden // chunks
    per = chunks // experts
    for e in range(experts):
        taken = sorted_rows[e * per * rows : (e + 1) * per * rows].astype(bf16)
        gate, up = dot(taken, gate_ref[e]), dot(taken, up_ref[e])
        for q in range(per):
            j = e * per + q
            cut = slice(q * rows, (q + 1) * rows)
            out_ref[j, :, 0:hidden] = gate[cut].astype(bf16)
            out_ref[j, :, hidden : 2 * hidden] = up[cut].astype(bf16)
            tile = j * share // lanes * lanes
            turn = j * share % lanes
            g = pltpu.roll(shared_gate[:, tile : tile + lanes], (lanes - turn) % lanes, 1)
            u = pltpu.roll(shared_up[:, tile : tile + lanes], (lanes + share - turn) % lanes, 1)
            whole = slice(j * rows, (j + 1) * rows)
            last = jnp.where(lane < share, g, jnp.where(lane < 2 * share, u, 0.0))
            last = jnp.where(lane == 2 * share, high[whole], last)
            last = jnp.where(lane == 2 * share + 1, low[whole], last)
            last = jnp.where(lane == 2 * share + 2, own_high, last)
            last = jnp.where(lane == 2 * share + 3, own_low, last)
            out_ref[j, :, 2 * hidden :] = last.astype(bf16)


def activate(got_ref, inner_ref, own_ref, width):
    chunks, rows, _ = got_ref.shape
    hidden = inner_ref.shape[1] - lanes
    share = hidden // chunks
    total = jnp.sum(got_ref[...].astype(f32), axis=0)
    last = total[:, 2 * hidden :]

    def inv_std(at):
        squares = last[:, at : at + 1] + last[:, at + 1 : at + 2]
        return lax.rsqrt(squares / width + norm_eps)

    inv = inv_std(2 * share)
    gate = rounded(total[:, :hidden] * inv)
    up = rounded(total[:, hidden : 2 * hidden] * inv)
    inner_ref[:, :hidden] = (silu(gate) * up).astype(bf16)
    inv = inv_std(2 * share + 2)
    own_ref[...] = jnp.broadcast_to(inv, own_ref.shape)
    both = rounded(last * inv)
    up = pltpu.roll(both, lanes - share, 1)
    lane = iota((rows, lanes), 1)
    inner_ref[:, hidden:] = jnp.where(lane < share, silu(both) * up, 0.0).astype(bf16)


def contract(inner_ref, back_ref, down_ref, out_ref):
    experts, hidden, _ = down_ref.shape
    per = inner_ref.shape[0] // experts
    outs = [
        dot(inner_ref[e * per : (e + 1) * per, :hidden], down_ref[e]).astype(bf16)
        for e in range(experts)
    ]
    out_ref[...] = dot(back_ref[...], jnp.concatenate(outs, axis=0)).astype(bf16)


def share_out(inner_ref, down_ref, centred_ref, gain_ref, inv_ref, behind, base_ref):
    chunks, _, width = inner_ref.shape
    hidden = width - lanes
    share = hidden // chunks
    normed = rounded(centred_ref[...] * inv_ref[...] * gain_ref[...])
    total = res_scale * normed
    for j in range(chunks):
        total += dot(
            inner_ref[j, :, hidden : hidden + share], down_ref[j * share : (j + 1) * share]
        )
    base_ref[...] = total


def combine(got_ref, high_ref, low_ref, base_ref, resid_ref, stats_ref):
    got = got_ref[...]
    resid = base_ref[...] + dot(high_ref[...], got) + dot(low_ref[...], got)
    resid_ref[...] = resid
    sums = as_row(jnp.sum(resid, axis=1, keepdims=True))
    squares = as_row(jnp.sum(resid * resid, axis=1, keepdims=True))
    at = iota((8, lanes), 0)
    tile = jnp.where(at == 0, sums, jnp.where(at == 1, squares, 0.0))
    for j in range(stats_ref.shape[0]):
        stats_ref[j] = tile


def finish(got_ref, resid_ref, gain_ref, out_ref, width):
    rows = resid_ref.shape[0]
    total = jnp.sum(got_ref[...], axis=0)
    mean = as_column(total[0:1], rows) / width
    spread = as_column(total[1:2], rows) / width - mean * mean
    out_ref[...] = (
        (resid_ref[...] - mean) * lax.rsqrt(spread + norm_eps) * gain_ref[...]
    ).astype(bf16)


def to_each(value, axis):
    return lax.all_to_all(value, axis, split_axis=0, concat_axis=0, tiled=True)


def per_device(
    tokens,
    state,
    w_query,
    w_key,
    w_value,
    w_outgate,
    decay_down,
    decay_up,
    decay_bias,
    head_gain,
    w_output,
    norm1_gain,
    route_ids,
    route_weight,
    exp_gate,
    exp_up,
    exp_down,
    sh_gate,
    sh_up,
    sh_down,
    norm2_gain,
):
    rows, width = tokens.shape
    tp_count, ep_count = lax.axis_size("tp"), lax.axis_size("ep")
    cols = width // tp_count
    hidden = exp_gate.shape[2]
    per_block = exp_gate.shape[0] * capacity
    slots = ep_count * per_block
    gain1, gain2 = norm1_gain.reshape(1, cols), norm2_gain.reshape(1, cols)

    outgoing = local_call(
        attend,
        struct((tp_count, rows + 8, cols), bf16),
        (
            tokens,
            state,
            w_query,
            w_key,
            w_value,
            w_outgate,
            decay_down,
            decay_up,
            decay_bias.reshape(1, -1),
            head_gain.reshape(1, -1),
            w_output,
        ),
    )
    arrived = to_each(outgoing, "tp")
    turned = jnp.pad(route_ids.T, ((0, 2), (0, lanes - rows)), constant_values=-1)
    send, high, low, perm, back = local_call(
        place,
        (
            struct((slots, lanes), bf16),
            struct((rows, slots), bf16),
            struct((rows, slots), bf16),
            struct((slots, slots), bf16),
            struct((slots, slots), bf16),
        ),
        (route_ids, turned, route_weight, outgoing),
        unread=1,
    )
    own_tokens = lax.dynamic_slice_in_dim(tokens, lax.axis_index("tp") * cols, cols, 1)
    sent, centred = local_call(
        dispatch,
        (struct((slots, cols), bf16), struct((rows, cols), f32)),
        (arrived, tokens, own_tokens, gain1, send),
    )
    taken = to_each(sent.reshape(ep_count, per_block, cols), "ep").reshape(slots, cols)
    partials = local_call(
        expand,
        struct((tp_count, rows, 2 * hidden + lanes), bf16),
        (taken, perm, exp_gate, exp_up, sh_gate, sh_up, gain1, centred),
    )
    parts = to_each(partials, "tp")

    def activate_rows(*refs):
        activate(*refs, width)

    activate_rows.__name__ = "activate"
    inner, inv = local_call(
        activate_rows,
        (struct((rows, hidden + lanes), bf16), struct((rows, cols), f32)),
        (parts,),
    )
    inners = lax.all_gather(inner, "tp", axis=0, tiled=True)
    result = local_call(contract, struct((slots, cols), bf16), (inners, back, exp_down))
    returned = to_each(result.reshape(ep_count, per_block, cols), "ep").reshape(slots, cols)
    base = local_call(
        share_out,
        struct((rows, cols), f32),
        (inners.reshape(tp_count, rows, -1), sh_down, centred, gain1, inv, result),
        unread=1,
    )
    resid, stats = local_call(
        combine,
        (struct((rows, cols), f32), struct((tp_count, 8, lanes), f32)),
        (returned, high, low, base),
    )
    all_stats = to_each(stats, "tp")

    def finish_rows(*refs):
        finish(*refs, width)

    finish_rows.__name__ = "finish"
    return local_call(finish_rows, struct((rows, cols), bf16), (all_stats, resid, gain2))


def solution(mesh):
    in_specs = (
        P("ep", None),
        P("ep", "tp", None, None),
        P(None, "tp"),
        P(None, "tp"),
        P(None, "tp"),
        P(None, "tp"),
        P(),
        P(None, "tp"),
        P("tp"),
        P(),
        P("tp", None),
        P("tp"),
        P("ep", None),
        P("ep", None),
        P("ep", "tp", None),
        P("ep", "tp", None),
        P("ep", None, "tp"),
        P("tp", None),
        P("tp", None),
        P(None, "tp"),
        P("tp"),
    )
    out_specs = P("ep", "tp")
    return jax.shard_map(
        per_device, mesh=mesh, in_specs=in_specs, out_specs=out_specs, check_vma=False
    )
```

time: 234 us -> 150 us (0.64)
  waiting for transfers between devices: 78.6 us -> 13.9 us
  blocking collectives: 31.1 us -> 87.7 us
  local copies, waits for them, and re-layouts: 36.5 us -> 6.38 us
  starting transfers between devices: 46.1 us -> 18.3 us
  Pallas kernels: 0 us -> 22.7 us
  matrix products: 17.8 us -> 0 us
  between operations: 13.7 us -> 0.03 us
  other arithmetic: 8.71 us -> 0 us
    all_to_all x1 -> x3, blocking collectives: 14.1 us -> 70.2 us  [to_each(): return lax.all_to_all(value, axis, split_axis=0, concat_axis=0, tiled=True)]
    reduce_scatter x1 -> x0, waiting for transfers between devices: 51.9 us -> none  [one_scatter(): lax.psum_scatter(lines, axis, tiled=True).reshape(-1)]
    all_to_all x4 -> x2, starting transfers between devices: 45.9 us -> 18.3 us  [to_each(): return lax.all_to_all(value, axis, split_axis=0, concat_axis=0, tiled=True)]
    pallas_call x0 -> x9, Pallas kernels: none -> 22.7 us  [local_call(): pl.pallas_call(body, out_shape=outs, in_specs=[vmem] * (len(args) - unrea...]
    reshape x19 -> x0, local copies, waits for them, and re-layouts: 18.1 us -> none  [the longest x4 8.34 us: one_scatter(): lines = jnp.concatenate([b.reshape(size, -1) for b in tiles], axis=1)]
    dot_general x16 -> x0, matrix products: 17.8 us -> none  [the longest x10 9.38 us: project(): return jnp.dot(left, right, preferred_element_type=jnp.float32)]
    all_to_all x4 -> x2, waiting for transfers between devices: 26.7 us -> 13.9 us  [to_each(): return lax.all_to_all(value, axis, split_axis=0, concat_axis=0, tiled=True)]
    transpose x4 -> x0, local copies, waits for them, and re-layouts: 8.55 us -> none  [the longest x2 8.35 us: split_up(): return jnp.moveaxis(value.reshape(*before, size, -1, *after), dim, 0)]
  transfers between devices with their start and end apart: 5 -> 2, of which waited for: 5 -> 2; matrix products, arithmetic and copies ran while one was open for 5% -> 2% of each run, Pallas kernels for 0% -> 3%
where the time goes in v1:
time: 150 us; the launch traced here: 149 us
  blocking collectives  87.7 us (58%)
  Pallas kernels  22.7 us (15%)
  starting transfers between devices  18.3 us (12%)
  waiting for transfers between devices  13.9 us (9%)
  local copies, waits for them, and re-layouts  6.38 us (4%)
    all_to_all x3, blocking collectives, to_each(): return lax.all_to_all(value, axis, split_axis=0, concat_axis=0, tiled=True)  70.2 us
    pallas_call x9, Pallas kernels, local_call(): pl.pallas_call(body, out_shape=outs, in_specs=[vmem] * (len(args) - unrea...  22.7 us
    all_to_all x2, starting transfers between devices, to_each(): return lax.all_to_all(value, axis, split_axis=0, concat_axis=0, tiled=True)  18.3 us
    all_gather x1, blocking collectives, per_device(): inners = lax.all_gather(inner, 'tp', axis=0, tiled=True)  17.4 us
    all_to_all x2, waiting for transfers between devices, to_each(): return lax.all_to_all(value, axis, split_axis=0, concat_axis=0, tiled=True)  13.9 us
    unnamed x11, local copies, waits for them, and re-layouts  4.49 us
  transfers between devices with their start and end apart: 2, of which 2 were waited for; matrix products, arithmetic and copies ran while one was open for 2% of the time, Pallas kernels for 3%

profile of v1, /device:TPU:1, one launch (start us, length us, event | category | flops | bytes accessed | tf_op | source)
XLA Modules:
  0.0 148.9 jit_solution(17126354144702529574)
XLA Ops:
  0.0 1.8 %copy.22.dd_ref = bf16[2048,16]{1,0:T(8,128)(2,1)} copy(bf16[2048,16]{0,1:T(8,128)(2,1)} %param.27) | data formatting | bytes 131072 | tf_op args[6]
  1.8 0.0 copy-start.3
  1.8 0.0 copy-start.2
  1.8 6.1 %attend.1.behind = bf16[16,32,128]{2,1,0:T(8,128)(2,1)} custom-call(bf16[24,2048]{1,0:T(8,128)(2,1)} %tok_ref.3, f32[24,1,128,256]{3,2,1,0:T(8,128)} %state_ref.1, bf16[2048,128]{1,0:T(8,128)(2,1)} %wq_ref.1, bf16[2048,128]{1,0:T(8,128)(2,1)} %wk_ref.1, bf16[2048,256]{1,0:T(8,128)(2,1)} %wv_ref.1, bf16[2048,256]{1,0:T(8,128)(2,1)} %wg_ref.1, ...), custom_call_target="tpu_custom_call" | custom-call | tf_op jit(solution)/shard_map/attend/pallas_call | solution.py:21
  8.0 13.8 %all-to-all-start = ((bf16[16,32,128]{2,1,0:T(8,128)(2,1)}), bf16[16,32,128]{2,1,0:T(8,128)(2,1)S(1)}, u32[]{:S(2)}, u32[]{:S(2)}) async-start(bf16[16,32,128]{2,1,0:T(8,128)(2,1)} %attend.1.behind), calls=%async_computation | async-start | bytes 262144 | tf_op jit(solution)/shard_map/all_to_all | solution.py:256
  21.7 0.0 copy-done.3
  21.7 0.7 copy.24.weight_ref
  22.4 0.0 copy-done.2
  22.4 0.7 copy.23.ids_ref
  23.1 0.6 pad.4.turned_ref
  23.7 2.1 %place.1 = (bf16[384,128]{1,0:T(8,128)(2,1)}, bf16[24,384]{1,0:T(8,128)(2,1)}, bf16[24,384]{1,0:T(8,128)(2,1)}, bf16[384,384]{1,0:T(8,128)(2,1)}, bf16[384,384]{1,0:T(8,128)(2,1)}) custom-call(s32[24,6]{1,0:T(8,128)} %copy.23.ids_ref, s32[8,128]{1,0:T(8,128)} %pad.4.turned_ref, f32[24,6]{1,0:T(8,128)} %copy.24.weight_ref, bf16[16,32,128]{2,1,0:T(8,128)(2,1)} %attend.1.behind), custom_call_target="tpu_custom_call" | custom-call | tf_op jit(solution)/shard_map/place/pallas_call | solution.py:21
  25.8 1.3 constant_dynamic-slice_fusion.own_ref
  27.1 3.8 %all-to-all-done.got_ref = bf16[16,32,128]{2,1,0:T(8,128)(2,1)S(1)} async-done(((bf16[16,32,128]{2,1,0:T(8,128)(2,1)}), bf16[16,32,128]{2,1,0:T(8,128)(2,1)S(1)}, u32[]{:S(2)}, u32[]{:S(2)}) %all-to-all-start) | async-done | bytes 131104 | tf_op jit(solution)/shard_map/all_to_all | solution.py:256
  30.9 0.0 copy-start
  30.9 0.7 copy-done
  31.6 1.9 %dispatch.1 = (bf16[384,128]{1,0:T(8,128)(2,1)}, f32[24,128]{1,0:T(8,128)}) custom-call(bf16[16,32,128]{2,1,0:T(8,128)(2,1)} %copy-done, bf16[24,2048]{1,0:T(8,128)(2,1)} %tok_ref.3, bf16[24,128]{1,0:T(8,128)(2,1)} %constant_dynamic-slice_fusion.own_ref, f32[1,128]{1,0:T(1,128)} %bitcast.16, bf16[384,128]{1,0:T(8,128)(2,1)} %get-tuple-element.16.send_ref), custom_call_target="tpu_custom_call" | custom-call | tf_op jit(solution)/shard_map/dispatch/pallas_call | solution.py:21
  33.5 24.6 %all_to_all.25 = bf16[48,8,128]{2,1,0:T(8,128)(2,1)} all-to-all(bf16[48,8,128]{2,1,0:T(8,128)(2,1)} %bitcast.14), channel_id=1, replica_groups=mesh['ep'=48,'tp'=16] {'ep'}, dimensions={0} | all-to-all | bytes 196608 | tf_op jit(solution)/shard_map/all_to_all | solution.py:256
  58.1 2.8 %expand.1 = bf16[16,24,1152]{2,1,0:T(8,128)(2,1)} custom-call(bf16[384,128]{1,0:T(8,128)(2,1)} %bitcast.12, bf16[384,384]{1,0:T(8,128)(2,1)} %get-tuple-element.18.perm_ref, bf16[4,128,512]{2,1,0:T(8,128)(2,1)} %gate_ref.1, bf16[4,128,512]{2,1,0:T(8,128)(2,1)} %up_ref.1, bf16[128,512]{1,0:T(8,128)(2,1)} %sg_ref.1, bf16[128,512]{1,0:T(8,128)(2,1)} %su_ref.1, ...), custom_call_target="tpu_custom_call" | custom-call | tf_op jit(solution)/shard_map/expand/pallas_call | solution.py:21
  60.9 31.1 %all_to_all.26.refs_0_ = bf16[16,24,1152]{2,1,0:T(8,128)(2,1)} all-to-all(bf16[16,24,1152]{2,1,0:T(8,128)(2,1)} %expand.1), channel_id=1, replica_groups=mesh['ep'=48,'tp'=16] {'tp'}, dimensions={0} | all-to-all | bytes 1769472 | tf_op jit(solution)/shard_map/all_to_all | solution.py:256
  92.1 2.1 %activate.1 = (bf16[24,640]{1,0:T(8,128)(2,1)}, f32[24,128]{1,0:T(8,128)}) custom-call(bf16[16,24,1152]{2,1,0:T(8,128)(2,1)} %all_to_all.26.refs_0_), custom_call_target="tpu_custom_call" | custom-call | tf_op jit(solution)/shard_map/activate/pallas_call | solution.py:21
  94.1 17.4 %all_gather.3.inner_ref = bf16[384,640]{1,0:T(8,128)(2,1)} all-gather(bf16[24,640]{1,0:T(8,128)(2,1)} %get-tuple-element.20), channel_id=1, replica_groups=mesh['ep'=48,'tp'=16] {'tp'}, dimensions={0}, use_global_device_ids=true | all-gather | bytes 522240 | tf_op jit(solution)/shard_map/all_gather | solution.py:344
  111.6 2.4 %contract.1.behind = bf16[384,128]{1,0:T(8,128)(2,1)} custom-call(bf16[384,640]{1,0:T(8,128)(2,1)} %all_gather.3.inner_ref, bf16[384,384]{1,0:T(8,128)(2,1)} %get-tuple-element.21.back_ref, bf16[4,512,128]{2,1,0:T(8,128)(2,1)} %down_ref.2), custom_call_target="tpu_custom_call" | custom-call | tf_op jit(solution)/shard_map/contract/pallas_call | solution.py:21
  113.9 4.5 %all-to-all-start.3 = ((bf16[48,8,128]{2,1,0:T(8,128)(2,1)}), bf16[48,8,128]{2,1,0:T(8,128)(2,1)S(1)}, u32[]{:S(2)}, u32[]{:S(2)}) async-start(bf16[48,8,128]{2,1,0:T(8,128)(2,1)} %bitcast.11), calls=%async_computation.3 | async-start | bytes 196608 | tf_op jit(solution)/shard_map/all_to_all | solution.py:256
  118.5 1.9 %share_out.1.base_ref = f32[24,128]{1,0:T(8,128)} custom-call(bf16[16,24,640]{2,1,0:T(8,128)(2,1)} %bitcast.10, bf16[512,128]{1,0:T(8,128)(2,1)} %down_ref.3, f32[24,128]{1,0:T(8,128)} %get-tuple-element.19.centred_ref, f32[1,128]{1,0:T(1,128)} %bitcast.18, f32[24,128]{1,0:T(8,128)} %get-tuple-element.24.inv_ref, bf16[384,128]{1,0:T(8,128)(2,1)} %contract.1.behind), custom_call_target="tpu_custom_call" | custom-call | tf_op jit(solution)/shard_map/share_out/pallas_call | solution.py:21
  120.4 10.0 %all-to-all-done.3 = bf16[48,8,128]{2,1,0:T(8,128)(2,1)S(1)} async-done(((bf16[48,8,128]{2,1,0:T(8,128)(2,1)}), bf16[48,8,128]{2,1,0:T(8,128)(2,1)S(1)}, u32[]{:S(2)}, u32[]{:S(2)}) %all-to-all-start.3) | async-done | bytes 98336 | tf_op jit(solution)/shard_map/all_to_all | solution.py:256
  130.4 0.0 copy-start.1
  130.4 0.6 copy-done.1
  131.0 1.8 %combine.1 = (f32[24,128]{1,0:T(8,128)}, f32[16,8,128]{2,1,0:T(8,128)}) custom-call(bf16[384,128]{1,0:T(8,128)(2,1)} %bitcast.13, bf16[24,384]{1,0:T(8,128)(2,1)} %get-tuple-element.22.high_ref, bf16[24,384]{1,0:T(8,128)(2,1)} %get-tuple-element.23.low_ref, f32[24,128]{1,0:T(8,128)} %share_out.1.base_ref), custom_call_target="tpu_custom_call" | custom-call | tf_op jit(solution)/shard_map/combine/pallas_call | solution.py:21
  132.8 14.5 %all_to_all.27.refs_0_ = f32[16,8,128]{2,1,0:T(8,128)} all-to-all(f32[16,8,128]{2,1,0:T(8,128)} %get-tuple-element.25), channel_id=1, replica_groups=mesh['ep'=48,'tp'=16] {'tp'}, dimensions={0} | all-to-all | bytes 131072 | tf_op jit(solution)/shard_map/all_to_all | solution.py:256
  147.3 1.6 %finish.1 = bf16[24,128]{1,0:T(8,128)(2,1)} custom-call(f32[16,8,128]{2,1,0:T(8,128)} %all_to_all.27.refs_0_, f32[24,128]{1,0:T(8,128)} %get-tuple-element.26.refs_1_, f32[1,128]{1,0:T(1,128)} %bitcast.21), custom_call_target="tpu_custom_call" | custom-call | tf_op jit(solution)/shard_map/finish/pallas_call | solution.py:21
Async XLA Ops:
  1.8 19.9 %copy-start.3 = (f32[24,6]{0,1:T(8,128)S(1)}, f32[24,6]{0,1:T(8,128)}, u32[]{:S(2)}) copy-start(f32[24,6]{0,1:T(8,128)} %param.34) | copy-start | bytes 1732
  1.8 20.6 %copy-start.2 = (s32[24,6]{0,1:T(8,128)S(1)}, s32[24,6]{0,1:T(8,128)}, u32[]{:S(2)}) copy-start(s32[24,6]{0,1:T(8,128)} %param.33) | copy-start | bytes 1732
  8.0 23.0 %all-to-all-start = ((bf16[16,32,128]{2,1,0:T(8,128)(2,1)}), bf16[16,32,128]{2,1,0:T(8,128)(2,1)S(1)}, u32[]{:S(2)}, u32[]{:S(2)}) async-start(bf16[16,32,128]{2,1,0:T(8,128)(2,1)} %attend.1.behind), calls=%async_computation | async-start | bytes 262144 | tf_op jit(solution)/shard_map/all_to_all | solution.py:256
  30.9 0.7 copy-start
  113.9 16.4 %all-to-all-start.3 = ((bf16[48,8,128]{2,1,0:T(8,128)(2,1)}), bf16[48,8,128]{2,1,0:T(8,128)(2,1)S(1)}, u32[]{:S(2)}, u32[]{:S(2)}) async-start(bf16[48,8,128]{2,1,0:T(8,128)(2,1)} %bitcast.11), calls=%async_computation.3 | async-start | bytes 196608 | tf_op jit(solution)/shard_map/all_to_all | solution.py:256
  130.4 0.6 copy-start.1

commit v2 on v1

--- a/solution.py
+++ b/solution.py
@@ -15,20 +15,26 @@
 bf16 = jnp.bfloat16
 
 
-def local_call(body, outs, args, unread=0):
+def local_call(body, outs, args, stay=(), scratch=()):
     vmem = pl.BlockSpec(memory_space=pltpu.VMEM)
-    anywhere = pl.BlockSpec(memory_space=pl.ANY)
+    hbm = pl.BlockSpec(memory_space=pl.ANY)
+    placed = [
+        pltpu.with_memory_space_constraint(a, pltpu.HBM if k in stay else pltpu.VMEM)
+        for k, a in enumerate(args)
+    ]
     return pl.pallas_call(
         body,
         out_shape=outs,
-        in_specs=[vmem] * (len(args) - unread) + [anywhere] * unread,
+        in_specs=[hbm if k in stay else vmem for k in range(len(args))],
         out_specs=jax.tree.map(lambda _: vmem, outs),
+        scratch_shapes=scratch,
+        compiler_params=pltpu.CompilerParams(vmem_limit_bytes=24 * 2**20),
         name=body.__name__,
-    )(*args)
+    )(*placed)
 
 
 def struct(shape, dtype):
-    return jax.ShapeDtypeStruct(shape, dtype)
+    return pltpu.VMEM(shape, dtype)
 
 
 def iota(shape, dim):
@@ -59,30 +65,97 @@
 
 
 def attend(
-    tok_ref, state_ref, wq_ref, wk_ref, wv_ref, wg_ref, dd_ref, du_ref, db_ref, hg_ref, wo_ref, out_ref
+    tok_hbm,
+    wq_hbm,
+    dd_hbm,
+    du_hbm,
+    state_hbm,
+    wk_hbm,
+    wv_hbm,
+    wg_hbm,
+    wo_hbm,
+    db_hbm,
+    hg_hbm,
+    out_ref,
+    done_ref,
+    tok_ref,
+    wq_ref,
+    dd_ref,
+    du_ref,
+    state_ref,
+    wk_ref,
+    wv_ref,
+    wg_ref,
+    wo_ref,
+    db_ref,
+    hg_ref,
+    sems,
 ):
     rows = tok_ref.shape[0]
     key_dim = wq_ref.shape[1]
+    parts = sems.shape[0] - 10
+    step = rows // parts
+    copies = [
+        pltpu.make_async_copy(a, b, sems.at[k])
+        for k, (a, b) in enumerate(
+            (
+                (tok_hbm, tok_ref),
+                (wq_hbm, wq_ref),
+                (dd_hbm, dd_ref),
+                (du_hbm, du_ref),
+                (db_hbm, db_ref),
+                (hg_hbm, hg_ref),
+            )
+        )
+    ]
+    pieces = [
+        pltpu.make_async_copy(
+            state_hbm.at[pl.ds(p * step, step)], state_ref.at[pl.ds(p * step, step)], sems.at[10 + p]
+        )
+        for p in range(parts)
+    ]
+    later = [
+        pltpu.make_async_copy(a, b, sems.at[6 + k])
+        for k, (a, b) in enumerate(
+            ((wk_hbm, wk_ref), (wv_hbm, wv_ref), (wg_hbm, wg_ref), (wo_hbm, wo_ref))
+        )
+    ]
+    for copy in copies + pieces + later:
+        copy.start()
+    copies[0].wait()
+    copies[2].wait()
+    copies[3].wait()
+    copies[4].wait()
     tok = tok_ref[...]
-    queries = rounded(dot(tok, wq_ref[...])) * key_dim ** (-0.5)
-    keys = rounded(dot(tok, wk_ref[...]))
-    values = rounded(dot(tok, wv_ref[...]))
-    gate = rounded(dot(tok, wg_ref[...]))
-    low = dot(tok, dd_ref[...]).astype(bf16)
+    low = lax.dot_general(
+        tok, dd_ref[...], (((1,), (1,)), ((), ())), preferred_element_type=f32
+    ).astype(bf16)
     pre = dot(low, du_ref[...]) + db_ref[...]
     log_decay = (jnp.minimum(pre, 0.0) - jnp.log1p(jnp.exp(-jnp.abs(pre)))) / decay_tau
-    decayed = queries * jnp.exp(log_decay)
+    decay = jnp.exp(log_decay)
+    copies[1].wait()
+    queries = rounded(dot(tok, wq_ref[...])) * key_dim ** (-0.5)
+    decayed = queries * decay
     turned = jnp.concatenate([decayed, jnp.zeros((lanes - rows, key_dim), f32)], axis=0).T
-    carried = jnp.concatenate(
-        [
-            jnp.sum(turned[:, b : b + 1] * state_ref[b, 0], axis=0, keepdims=True)
-            for b in range(rows)
-        ],
-        axis=0,
-    )
+    carried = []
+    for p in range(parts):
+        pieces[p].wait()
+        for b in range(p * step, (p + 1) * step):
+            carried.append(
+                jnp.sum(turned[:, b : b + 1] * state_ref[b, 0], axis=0, keepdims=True)
+            )
+    carried = jnp.concatenate(carried, axis=0)
+    later[0].wait()
+    keys = rounded(dot(tok, wk_ref[...]))
+    later[1].wait()
+    values = rounded(dot(tok, wv_ref[...]))
+    later[2].wait()
+    gate = rounded(dot(tok, wg_ref[...]))
+    copies[5].wait()
     attended = carried + jnp.sum(queries * keys, axis=1, keepdims=True) * values
     inv_norm = lax.rsqrt(jnp.mean(attended * attended, axis=1, keepdims=True) + norm_eps)
     head_out = (attended * inv_norm * hg_ref[...] * silu(gate)).astype(bf16)
+    later[3].wait()
     partial = rounded(dot(head_out, wo_ref[...]))
     row = as_row(jnp.sum(partial, axis=1, keepdims=True))
     high = rounded(row)
@@ -94,26 +167,38 @@
         out_ref[j] = jnp.concatenate(
             [partial[:, j * lanes : (j + 1) * lanes], tail], axis=0
         ).astype(bf16)
-
-
-def place(ids_ref, turned_ref, weight_ref, behind, send_ref, high_ref, low_ref, perm_ref, back_ref):
-    rows, top = ids_ref.shape
+    done_ref[...] = tail
+
+
+def place(
+    ids_ref, weight_ref, tok_ref, behind, send_ref, high_ref, low_ref, perm_ref, back_ref, own_ref
+):
+    top, rows = ids_ref.shape
     slots = send_ref.shape[0]
     blocks = slots // (4 * capacity)
+
+    def square(ref):
+        wide = jnp.concatenate([ref[...].astype(f32), jnp.zeros((top, lanes - rows), f32)], axis=1)
+        return jnp.concatenate([wide, jnp.zeros((lanes - top, lanes), f32)], axis=0)
+
+    ids, weights = square(ids_ref), square(weight_ref)
     slot = iota((slots, lanes), 0)
+    expert = jnp.where(iota((slots, lanes), 1) < rows, slot // capacity, -1).astype(f32)
     hit = jnp.zeros((slots, lanes), f32)
     for k in range(top):
-        hit = jnp.where(turned_ref[k : k + 1, :] == slot // capacity, 1.0, hit)
+        hit = jnp.where(ids[k : k + 1, :] == expert, 1.0, hit)
     earlier = (iota((lanes, lanes), 0) < iota((lanes, lanes), 1)).astype(bf16)
     rank = dot(hit.astype(bf16), earlier)
     send_ref[...] = jnp.where(rank == (slot % capacity).astype(f32), hit, 0.0).astype(bf16)
+    ids, weights = ids.T, weights.T
     slot = iota((rows, slots), 1)
+    expert = (slot // capacity).astype(f32)
     hit = jnp.zeros((rows, slots), f32)
     weight = jnp.zeros((rows, slots), f32)
     for k in range(top):
-        same = ids_ref[:, k : k + 1] == slot // capacity
+        same = ids[:rows, k : k + 1] == expert
         hit = jnp.where(same, 1.0, hit)
-        weight = jnp.where(same, weight_ref[:, k : k + 1], weight)
+        weight = jnp.where(same, weights[:rows, k : k + 1], weight)
     earlier = (iota((rows, rows), 1) < iota((rows, rows), 0)).astype(bf16)
     rank = dot(earlier, hit.astype(bf16))
     weight = jnp.where(rank == (slot % capacity).astype(f32), weight, 0.0)
@@ -127,18 +212,20 @@
         return rest // capacity * (4 * capacity) + expert * capacity + rest % capacity
 
     one, two = iota((slots, slots), 0), iota((slots, slots), 1)
-    perm_ref[...] = (source(one) == two).astype(bf16)
-    back_ref[...] = (one == source(two)).astype(bf16)
-
-
-def dispatch(got_ref, tok_ref, own_ref, gain_ref, send_ref, rows_ref, centred_ref):
-    rows, width = tok_ref.shape
+    perm_ref[...] = (source(iota((slots, 1), 0)) == two).astype(bf16)
+    back_ref[...] = (one == source(iota((1, slots), 1))).astype(bf16)
+    width = tok_ref.shape[1]
+    start = pl.multiple_of(lax.axis_index("tp") * lanes, lanes)
+    mean = jnp.sum(tok_ref[...].astype(f32), axis=1, keepdims=True) / width
+    own_ref[...] = res_scale * (tok_ref[:, pl.ds(start, lanes)].astype(f32) - mean)
+
+
+def dispatch(got_ref, own_ref, gain_ref, send_ref, rows_ref, centred_ref, width):
+    rows = own_ref.shape[0]
     total = jnp.sum(got_ref[...].astype(f32), axis=0)
     mixed = rounded(total[:rows])
     sums = total[rows : rows + 1] + total[rows + 1 : rows + 2] + total[rows + 2 : rows + 3]
-    tok_sum = jnp.sum(tok_ref[...].astype(f32), axis=1, keepdims=True)
-    mean = (res_scale * tok_sum + as_column(sums, rows)) / width
-    centred = res_scale * own_ref[...].astype(f32) + mixed - mean
+    centred = own_ref[...] + mixed - as_column(sums, rows) / width
     centred_ref[...] = centred
     scaled = centred * gain_ref[...]
     filled = jnp.concatenate([scaled, jnp.zeros((lanes - rows, lanes), f32)], axis=0)
@@ -207,7 +294,7 @@
     inner_ref[:, hidden:] = jnp.where(lane < share, silu(both) * up, 0.0).astype(bf16)
 
 
-def contract(inner_ref, back_ref, down_ref, out_ref):
+def contract(inner_ref, back_ref, down_ref, out_ref, done_ref):
     experts, hidden, _ = down_ref.shape
     per = inner_ref.shape[0] // experts
     outs = [
@@ -215,6 +302,7 @@
         for e in range(experts)
     ]
     out_ref[...] = dot(back_ref[...], jnp.concatenate(outs, axis=0)).astype(bf16)
+    done_ref[...] = jnp.zeros(done_ref.shape, f32)
 
 
 def share_out(inner_ref, down_ref, centred_ref, gain_ref, inv_ref, behind, base_ref):
@@ -287,26 +375,28 @@
     slots = ep_count * per_block
     gain1, gain2 = norm1_gain.reshape(1, cols), norm2_gain.reshape(1, cols)
 
-    outgoing = local_call(
+    held = (
+        tokens,
+        w_query,
+        decay_down.T,
+        decay_up,
+        state,
+        w_key,
+        w_value,
+        w_outgate,
+        w_output,
+        decay_bias.reshape(1, -1),
+        head_gain.reshape(1, -1),
+    )
+    outgoing, done = local_call(
         attend,
-        struct((tp_count, rows + 8, cols), bf16),
-        (
-            tokens,
-            state,
-            w_query,
-            w_key,
-            w_value,
-            w_outgate,
-            decay_down,
-            decay_up,
-            decay_bias.reshape(1, -1),
-            head_gain.reshape(1, -1),
-            w_output,
-        ),
+        (struct((tp_count, rows + 8, cols), bf16), struct((8, cols), f32)),
+        held,
+        stay=tuple(range(len(held))),
+        scratch=[pltpu.VMEM(a.shape, a.dtype) for a in held] + [pltpu.SemaphoreType.DMA((13,))],
     )
     arrived = to_each(outgoing, "tp")
-    turned = jnp.pad(route_ids.T, ((0, 2), (0, lanes - rows)), constant_values=-1)
-    send, high, low, perm, back = local_call(
+    send, high, low, perm, back, own = local_call(
         place,
         (
             struct((slots, lanes), bf16),
@@ -314,15 +404,22 @@
             struct((rows, slots), bf16),
             struct((slots, slots), bf16),
             struct((slots, slots), bf16),
+            struct((rows, cols), f32),
         ),
-        (route_ids, turned, route_weight, outgoing),
-        unread=1,
-    )
-    own_tokens = lax.dynamic_slice_in_dim(tokens, lax.axis_index("tp") * cols, cols, 1)
+        (route_ids.T, route_weight.T, tokens, done),
+    )
+
+    def named(body):
+        def call(*refs):
+            body(*refs, width)
+
+        call.__name__ = body.__name__
+        return call
+
     sent, centred = local_call(
-        dispatch,
+        named(dispatch),
         (struct((slots, cols), bf16), struct((rows, cols), f32)),
-        (arrived, tokens, own_tokens, gain1, send),
+        (arrived, own, gain1, send),
     )
     taken = to_each(sent.reshape(ep_count, per_block, cols), "ep").reshape(slots, cols)
     partials = local_call(
@@ -332,23 +429,22 @@
     )
     parts = to_each(partials, "tp")
 
-    def activate_rows(*refs):
-        activate(*refs, width)
-
-    activate_rows.__name__ = "activate"
     inner, inv = local_call(
-        activate_rows,
+        named(activate),
         (struct((rows, hidden + lanes), bf16), struct((rows, cols), f32)),
         (parts,),
     )
     inners = lax.all_gather(inner, "tp", axis=0, tiled=True)
-    result = local_call(contract, struct((slots, cols), bf16), (inners, back, exp_down))
+    result, done = local_call(
+        contract,
+        (struct((slots, cols), bf16), struct((8, cols), f32)),
+        (inners, back, exp_down),
+    )
     returned = to_each(result.reshape(ep_count, per_block, cols), "ep").reshape(slots, cols)
     base = local_call(
         share_out,
         struct((rows, cols), f32),
-        (inners.reshape(tp_count, rows, -1), sh_down, centred, gain1, inv, result),
-        unread=1,
+        (inners.reshape(tp_count, rows, -1), sh_down, centred, gain1, inv, done),
     )
     resid, stats = local_call(
         combine,
@@ -357,11 +453,9 @@
     )
     all_stats = to_each(stats, "tp")
 
-    def finish_rows(*refs):
-        finish(*refs, width)
-
-    finish_rows.__name__ = "finish"
-    return local_call(finish_rows, struct((rows, cols), bf16), (all_stats, resid, gain2))
+    return local_call(
+        named(finish), jax.ShapeDtypeStruct((rows, cols), bf16), (all_stats, resid, gain2)
+    )
 
 
 def solution(mesh):

time: 150 us -> 132 us (0.88)
  Pallas kernels: 22.7 us -> 8.76 us
  local copies, waits for them, and re-layouts: 6.38 us -> 0.05 us
  waiting for transfers between devices: 13.9 us -> 20.2 us
  blocking collectives: 87.7 us -> 83.8 us
    pallas_call x9, Pallas kernels: 22.7 us -> 8.76 us  [local_call(): pl.pallas_call(body, out_shape=outs, in_specs=[hbm if k in stay else vmem...]
    all_to_all x2, waiting for transfers between devices: 13.9 us -> 20.2 us  [to_each(): return lax.all_to_all(value, axis, split_axis=0, concat_axis=0, tiled=True)]
    unnamed x11 -> x22, local copies, waits for them, and re-layouts: 4.49 us -> 0.05 us
    all_to_all x3, blocking collectives: 70.2 us -> 68 us  [to_each(): return lax.all_to_all(value, axis, split_axis=0, concat_axis=0, tiled=True)]
    all_gather x1, blocking collectives: 17.4 us -> 15.8 us  [per_device(): inners = lax.all_gather(inner, 'tp', axis=0, tiled=True)]
  transfers between devices with their start and end apart: 2 -> 2, of which waited for: 2 -> 2; matrix products, arithmetic and copies ran while one was open for 2% -> 0% of each run, Pallas kernels for 3% -> 1%
where the time goes in v2:
time: 132 us; the launch traced here: 131 us
  blocking collectives  83.8 us (63%)
  waiting for transfers between devices  20.2 us (15%)
  starting transfers between devices  18.3 us (14%)
  Pallas kernels  8.76 us (7%)
    all_to_all x3, blocking collectives, to_each(): return lax.all_to_all(value, axis, split_axis=0, concat_axis=0, tiled=True)  68 us
    all_to_all x2, waiting for transfers between devices, to_each(): return lax.all_to_all(value, axis, split_axis=0, concat_axis=0, tiled=True)  20.2 us
    all_to_all x2, starting transfers between devices, to_each(): return lax.all_to_all(value, axis, split_axis=0, concat_axis=0, tiled=True)  18.3 us
    all_gather x1, blocking collectives, per_device(): inners = lax.all_gather(inner, 'tp', axis=0, tiled=True)  15.8 us
    pallas_call x9, Pallas kernels, local_call(): pl.pallas_call(body, out_shape=outs, in_specs=[hbm if k in stay else vmem...  8.76 us
  transfers between devices with their start and end apart: 2, of which 2 were waited for; matrix products, arithmetic and copies ran while one was open for 0% of the time, Pallas kernels for 1%

profile of v2, /device:TPU:1, one launch (start us, length us, event | category | flops | bytes accessed | tf_op | source)
XLA Modules:
  0.0 131.2 jit_solution(2356415431850697161)
XLA Ops:
  0.0 0.0 copy-start.7
  0.0 0.0 copy-start.1
  0.0 0.0 copy-start.2
  0.0 0.0 copy-start.4
  0.0 0.0 copy-start.5
  0.1 4.8 %attend.1 = (bf16[16,32,128]{2,1,0:T(8,128)(2,1)}, f32[8,128]{1,0:T(8,128)S(1)}) custom-call(bf16[24,2048]{1,0:T(8,128)(2,1)} %tok_ref.1, bf16[2048,128]{1,0:T(8,128)(2,1)} %wq_hbm.1, bf16[16,2048]{1,0:T(8,128)(2,1)} %bitcast.22, bf16[16,128]{1,0:T(8,128)(2,1)} %du_hbm.1, f32[24,1,128,256]{3,2,1,0:T(8,128)} %state_hbm.1, bf16[2048,128]{1,0:T(8,128)(2,1)} %wk_hbm.1, ...), custom_call_target="tpu_custom_call" | custom-call | tf_op jit(solution)/shard_map/attend/pallas_call | solution.py:25
  4.9 13.8 %all-to-all-start = ((bf16[16,32,128]{2,1,0:T(8,128)(2,1)}), bf16[16,32,128]{2,1,0:T(8,128)(2,1)S(1)}, u32[]{:S(2)}, u32[]{:S(2)}) async-start(bf16[16,32,128]{2,1,0:T(8,128)(2,1)} %get-tuple-element.21), calls=%async_computation | async-start | bytes 262144 | tf_op jit(solution)/shard_map/all_to_all | solution.py:344
  18.6 0.0 copy-done.3
  18.6 0.0 copy-done.8
  18.6 0.0 copy-done.9
  18.7 0.0 copy-start
  18.7 0.7 place.1
  19.4 8.5 %all-to-all-done.refs_0_ = bf16[16,32,128]{2,1,0:T(8,128)(2,1)S(1)} async-done(((bf16[16,32,128]{2,1,0:T(8,128)(2,1)}), bf16[16,32,128]{2,1,0:T(8,128)(2,1)S(1)}, u32[]{:S(2)}, u32[]{:S(2)}) %all-to-all-start) | async-done | bytes 131104 | tf_op jit(solution)/shard_map/all_to_all | solution.py:344
  27.8 0.0 copy-done.7
  27.8 0.2 dispatch.1
  28.1 24.3 %all_to_all.25 = bf16[48,8,128]{2,1,0:T(8,128)(2,1)S(1)} all-to-all(bf16[48,8,128]{2,1,0:T(8,128)(2,1)S(1)} %bitcast.15), channel_id=1, replica_groups=mesh['ep'=48,'tp'=16] {'ep'}, dimensions={0} | all-to-all | bytes 196608 | tf_op jit(solution)/shard_map/all_to_all | solution.py:344
  52.4 0.0 copy-done.1
  52.4 0.0 copy-done.2
  52.4 0.0 copy-start.6
  52.4 0.5 expand.1
  52.9 0.0 copy-start.10
  53.0 29.4 %all_to_all.26.refs_0_ = bf16[16,24,1152]{2,1,0:T(8,128)(2,1)S(1)} all-to-all(bf16[16,24,1152]{2,1,0:T(8,128)(2,1)S(1)} %expand.1), channel_id=1, replica_groups=mesh['ep'=48,'tp'=16] {'tp'}, dimensions={0} | all-to-all | bytes 1769472 | tf_op jit(solution)/shard_map/all_to_all | solution.py:344
  82.4 0.3 activate.1
  82.7 15.8 %all_gather.3.inner_ref = bf16[384,640]{1,0:T(8,128)(2,1)S(1)} all-gather(bf16[24,640]{1,0:T(8,128)(2,1)S(1)} %get-tuple-element.28), channel_id=1, replica_groups=mesh['ep'=48,'tp'=16] {'tp'}, dimensions={0}, use_global_device_ids=true | all-gather | bytes 522240 | tf_op jit(solution)/shard_map/all_gather | solution.py:437
  98.5 1.1 contract.1
  99.6 4.5 %all-to-all-start.3 = ((bf16[48,8,128]{2,1,0:T(8,128)(2,1)}), bf16[48,8,128]{2,1,0:T(8,128)(2,1)S(1)}, u32[]{:S(2)}, u32[]{:S(2)}) async-start(bf16[48,8,128]{2,1,0:T(8,128)(2,1)} %bitcast.8), calls=%async_computation.3 | async-start | bytes 196608 | tf_op jit(solution)/shard_map/all_to_all | solution.py:344
  104.1 0.0 copy-done.6
  104.1 0.2 share_out.1.base_ref
  104.3 11.7 %all-to-all-done.3 = bf16[48,8,128]{2,1,0:T(8,128)(2,1)S(1)} async-done(((bf16[48,8,128]{2,1,0:T(8,128)(2,1)}), bf16[48,8,128]{2,1,0:T(8,128)(2,1)S(1)}, u32[]{:S(2)}, u32[]{:S(2)}) %all-to-all-start.3) | async-done | bytes 98336 | tf_op jit(solution)/shard_map/all_to_all | solution.py:344
  116.0 0.2 combine.1
  116.3 14.3 %all_to_all.27.refs_0_ = f32[16,8,128]{2,1,0:T(8,128)S(1)} all-to-all(f32[16,8,128]{2,1,0:T(8,128)S(1)} %get-tuple-element.35), channel_id=1, replica_groups=mesh['ep'=48,'tp'=16] {'tp'}, dimensions={0} | all-to-all | bytes 131072 | tf_op jit(solution)/shard_map/all_to_all | solution.py:344
  130.5 0.7 finish.1
  (7 shorter events, 0.0 us)
Async XLA Ops:
  0.0 18.6 %copy-start.3 = (bf16[24,2048]{1,0:T(8,128)(2,1)S(1)}, bf16[24,2048]{1,0:T(8,128)(2,1)}, u32[]{:S(2)}) copy-start(bf16[24,2048]{1,0:T(8,128)(2,1)} %tok_ref.1) | copy-start | bytes 294916
  0.0 18.6 %copy-start.8 = (s32[24,6]{0,1:T(8,128)S(1)}, s32[24,6]{0,1:T(8,128)}, u32[]{:S(2)}) copy-start(s32[24,6]{0,1:T(8,128)} %param.33) | copy-start | bytes 1732
  0.0 18.6 %copy-start.9 = (f32[24,6]{0,1:T(8,128)S(1)}, f32[24,6]{0,1:T(8,128)}, u32[]{:S(2)}) copy-start(f32[24,6]{0,1:T(8,128)} %param.34) | copy-start | bytes 1732
  0.0 27.8 %copy-start.7 = (f32[128]{0:T(128)S(1)}, f32[128]{0:T(128)}, u32[]{:S(2)}) copy-start(f32[128]{0:T(128)} %param.32) | copy-start | bytes 1540
  0.0 52.4 %copy-start.1 = (bf16[4,128,512]{2,1,0:T(8,128)(2,1)S(1)}, bf16[4,128,512]{2,1,0:T(8,128)(2,1)}, u32[]{:S(2)}) copy-start(bf16[4,128,512]{2,1,0:T(8,128)(2,1)} %gate_ref.1) | copy-start | bytes 1572868
  0.0 52.4 %copy-start.2 = (bf16[4,128,512]{2,1,0:T(8,128)(2,1)S(1)}, bf16[4,128,512]{2,1,0:T(8,128)(2,1)}, u32[]{:S(2)}) copy-start(bf16[4,128,512]{2,1,0:T(8,128)(2,1)} %up_ref.1) | copy-start | bytes 1572868
  0.0 52.4 %copy-start.4 = (bf16[128,512]{1,0:T(8,128)(2,1)S(1)}, bf16[128,512]{1,0:T(8,128)(2,1)}, u32[]{:S(2)}) copy-start(bf16[128,512]{1,0:T(8,128)(2,1)} %sg_ref.1) | copy-start | bytes 393220
  0.0 52.3 %copy-start.5 = (bf16[128,512]{1,0:T(8,128)(2,1)S(1)}, bf16[128,512]{1,0:T(8,128)(2,1)}, u32[]{:S(2)}) copy-start(bf16[128,512]{1,0:T(8,128)(2,1)} %su_ref.1) | copy-start | bytes 393220
  4.9 23.0 %all-to-all-start = ((bf16[16,32,128]{2,1,0:T(8,128)(2,1)}), bf16[16,32,128]{2,1,0:T(8,128)(2,1)S(1)}, u32[]{:S(2)}, u32[]{:S(2)}) async-start(bf16[16,32,128]{2,1,0:T(8,128)(2,1)} %get-tuple-element.21), calls=%async_computation | async-start | bytes 262144 | tf_op jit(solution)/shard_map/all_to_all | solution.py:344
  18.7 79.8 %copy-start = (bf16[4,512,128]{2,1,0:T(8,128)(2,1)S(1)}, bf16[4,512,128]{2,1,0:T(8,128)(2,1)}, u32[]{:S(2)}) copy-start(bf16[4,512,128]{2,1,0:T(8,128)(2,1)} %down_ref.2) | copy-start | bytes 1572868
  52.4 51.7 %copy-start.6 = (bf16[512,128]{1,0:T(8,128)(2,1)S(1)}, bf16[512,128]{1,0:T(8,128)(2,1)}, u32[]{:S(2)}) copy-start(bf16[512,128]{1,0:T(8,128)(2,1)} %down_ref.3) | copy-start | bytes 393220
  52.9 77.6 %copy-start.10 = (f32[128]{0:T(128)S(1)}, f32[128]{0:T(128)}, u32[]{:S(2)}) copy-start(f32[128]{0:T(128)} %param.41) | copy-start | bytes 1540
  99.6 16.4 %all-to-all-start.3 = ((bf16[48,8,128]{2,1,0:T(8,128)(2,1)}), bf16[48,8,128]{2,1,0:T(8,128)(2,1)S(1)}, u32[]{:S(2)}, u32[]{:S(2)}) async-start(bf16[48,8,128]{2,1,0:T(8,128)(2,1)} %bitcast.8), calls=%async_computation.3 | async-start | bytes 196608 | tf_op jit(solution)/shard_map/all_to_all | solution.py:344

commit v3 on v2

--- a/solution.py
+++ b/solution.py
@@ -64,115 +64,7 @@
     return value * jax.nn.sigmoid(value)
 
 
-def attend(
-    tok_hbm,
-    wq_hbm,
-    dd_hbm,
-    du_hbm,
-    state_hbm,
-    wk_hbm,
-    wv_hbm,
-    wg_hbm,
-    wo_hbm,
-    db_hbm,
-    hg_hbm,
-    out_ref,
-    done_ref,
-    tok_ref,
-    wq_ref,
-    dd_ref,
-    du_ref,
-    state_ref,
-    wk_ref,
-    wv_ref,
-    wg_ref,
-    wo_ref,
-    db_ref,
-    hg_ref,
-    sems,
-):
-    rows = tok_ref.shape[0]
-    key_dim = wq_ref.shape[1]
-    parts = sems.shape[0] - 10
-    step = rows // parts
-    copies = [
-        pltpu.make_async_copy(a, b, sems.at[k])
-        for k, (a, b) in enumerate(
-            (
-                (tok_hbm, tok_ref),
-                (wq_hbm, wq_ref),
-                (dd_hbm, dd_ref),
-                (du_hbm, du_ref),
-                (db_hbm, db_ref),
-                (hg_hbm, hg_ref),
-            )
-        )
-    ]
-    pieces = [
-        pltpu.make_async_copy(
-            state_hbm.at[pl.ds(p * step, step)], state_ref.at[pl.ds(p * step, step)], sems.at[10 + p]
-        )
-        for p in range(parts)
-    ]
-    later = [
-        pltpu.make_async_copy(a, b, sems.at[6 + k])
-        for k, (a, b) in enumerate(
-            ((wk_hbm, wk_ref), (wv_hbm, wv_ref), (wg_hbm, wg_ref), (wo_hbm, wo_ref))
-        )
-    ]
-    for copy in copies + pieces + later:
-        copy.start()
-    copies[0].wait()
-    copies[2].wait()
-    copies[3].wait()
-    copies[4].wait()
-    tok = tok_ref[...]
-    low = lax.dot_general(
-        tok, dd_ref[...], (((1,), (1,)), ((), ())), preferred_element_type=f32
-    ).astype(bf16)
-    pre = dot(low, du_ref[...]) + db_ref[...]
-    log_decay = (jnp.minimum(pre, 0.0) - jnp.log1p(jnp.exp(-jnp.abs(pre)))) / decay_tau
-    decay = jnp.exp(log_decay)
-    copies[1].wait()
-    queries = rounded(dot(tok, wq_ref[...])) * key_dim ** (-0.5)
-    decayed = queries * decay
-    turned = jnp.concatenate([decayed, jnp.zeros((lanes - rows, key_dim), f32)], axis=0).T
-    carried = []
-    for p in range(parts):
-        pieces[p].wait()
-        for b in range(p * step, (p + 1) * step):
-            carried.append(
-                jnp.sum(turned[:, b : b + 1] * state_ref[b, 0], axis=0, keepdims=True)
-            )
-    carried = jnp.concatenate(carried, axis=0)
-    later[0].wait()
-    keys = rounded(dot(tok, wk_ref[...]))
-    later[1].wait()
-    values = rounded(dot(tok, wv_ref[...]))
-    later[2].wait()
-    gate = rounded(dot(tok, wg_ref[...]))
-    copies[5].wait()
-    attended = carried + jnp.sum(queries * keys, axis=1, keepdims=True) * values
-    inv_norm = lax.rsqrt(jnp.mean(attended * attended, axis=1, keepdims=True) + norm_eps)
-    head_out = (attended * inv_norm * hg_ref[...] * silu(gate)).astype(bf16)
-    later[3].wait()
-    partial = rounded(dot(head_out, wo_ref[...]))
-    row = as_row(jnp.sum(partial, axis=1, keepdims=True))
-    high = rounded(row)
-    middle = rounded(row - high)
-    low = row - high - middle
-    at = iota((8, lanes), 0)
-    tail = jnp.where(at == 0, high, jnp.where(at == 1, middle, jnp.where(at == 2, low, 0.0)))
-    for j in range(out_ref.shape[0]):
-        out_ref[j] = jnp.concatenate(
-            [partial[:, j * lanes : (j + 1) * lanes], tail], axis=0
-        ).astype(bf16)
-    done_ref[...] = tail
-
-
-def place(
-    ids_ref, weight_ref, tok_ref, behind, send_ref, high_ref, low_ref, perm_ref, back_ref, own_ref
-):
+def route(ids_ref, weight_ref, send_ref, high_ref, low_ref, perm_ref, back_ref):
     top, rows = ids_ref.shape
     slots = send_ref.shape[0]
     blocks = slots // (4 * capacity)
@@ -214,10 +106,68 @@
     one, two = iota((slots, slots), 0), iota((slots, slots), 1)
     perm_ref[...] = (source(iota((slots, 1), 0)) == two).astype(bf16)
     back_ref[...] = (one == source(iota((1, slots), 1))).astype(bf16)
-    width = tok_ref.shape[1]
+
+
+def attend(*refs):
+    count = 13
+    far, out_ref, tables, own_ref = refs[:count], refs[count], refs[count + 1 : count + 6], refs[count + 6]
+    near, sems = refs[count + 7 : -1], refs[-1]
+    ids, weights, tok, dd, du, db, wq, wk, wv, wg, hg, state, wo = range(count)
+    copies = [pltpu.make_async_copy(a, b, sems.at[k]) for k, (a, b) in enumerate(zip(far, near))]
+    for copy in copies:
+        copy.start()
+
+    def ready(*which):
+        for k in which:
+            copies[k].wait()
+
+    ready(ids, weights)
+    route(near[ids], near[weights], *tables)
+    ready(tok, dd, du, db)
+    tok_ref = near[tok]
+    rows, width = tok_ref.shape
+    tokens = tok_ref[...]
     start = pl.multiple_of(lax.axis_index("tp") * lanes, lanes)
-    mean = jnp.sum(tok_ref[...].astype(f32), axis=1, keepdims=True) / width
+    mean = jnp.sum(tokens.astype(f32), axis=1, keepdims=True) / width
     own_ref[...] = res_scale * (tok_ref[:, pl.ds(start, lanes)].astype(f32) - mean)
+    low = lax.dot_general(
+        tokens, near[dd][...], (((1,), (1,)), ((), ())), preferred_element_type=f32
+    ).astype(bf16)
+    pre = dot(low, near[du][...]) + near[db][...]
+    log_decay = (jnp.minimum(pre, 0.0) - jnp.log1p(jnp.exp(-jnp.abs(pre)))) / decay_tau
+    decay = jnp.exp(log_decay)
+    ready(wq)
+    key_dim = near[wq].shape[1]
+    queries = rounded(dot(tokens, near[wq][...])) * key_dim ** (-0.5)
+    decayed = queries * decay
+    turned = jnp.concatenate([decayed, jnp.zeros((lanes - rows, key_dim), f32)], axis=0).T
+    ready(wk, wv)
+    keys = rounded(dot(tokens, near[wk][...]))
+    values = rounded(dot(tokens, near[wv][...]))
+    ready(wg, hg, state)
+    gate = rounded(dot(tokens, near[wg][...]))
+    carried = jnp.concatenate(
+        [
+            jnp.sum(turned[:, b : b + 1] * near[state][b, 0], axis=0, keepdims=True)
+            for b in range(rows)
+        ],
+        axis=0,
+    )
+    attended = carried + jnp.sum(queries * keys, axis=1, keepdims=True) * values
+    inv_norm = lax.rsqrt(jnp.mean(attended * attended, axis=1, keepdims=True) + norm_eps)
+    head_out = (attended * inv_norm * near[hg][...] * silu(gate)).astype(bf16)
+    ready(wo)
+    partial = rounded(dot(head_out, near[wo][...]))
+    row = as_row(jnp.sum(partial, axis=1, keepdims=True))
+    high = rounded(row)
+    middle = rounded(row - high)
+    low = row - high - middle
+    at = iota((8, lanes), 0)
+    tail = jnp.where(at == 0, high, jnp.where(at == 1, middle, jnp.where(at == 2, low, 0.0)))
+    for j in range(out_ref.shape[0]):
+        out_ref[j] = jnp.concatenate(
+            [partial[:, j * lanes : (j + 1) * lanes], tail], axis=0
+        ).astype(bf16)
 
 
 def dispatch(got_ref, own_ref, gain_ref, send_ref, rows_ref, centred_ref, width):
@@ -237,9 +187,13 @@
     return high, column - high
 
 
-def expand(rows_ref, perm_ref, gate_ref, up_ref, sg_ref, su_ref, gain_ref, centred_ref, out_ref):
-    chunks, rows, width = out_ref.shape
+def expand(
+    rows_ref, perm_ref, gate_ref, up_ref, sg_ref, su_ref, gain_ref, centred_ref, keep_ref, send_ref
+):
+    pairs, rows, _ = keep_ref.shape
     experts, _, hidden = gate_ref.shape
+    chunks = 2 * pairs
+    even = lax.rem(lax.axis_index("tp"), 2) == 0
     sorted_rows = dot(perm_ref[...], rows_ref[...])
     scale = sorted_rows / gain_ref[...]
     high, low = two_parts(jnp.sum(scale * scale, axis=1, keepdims=True))
@@ -250,29 +204,51 @@
     lane = iota((rows, lanes), 1)
     share = hidden // chunks
     per = chunks // experts
+
+    def last_block(j):
+        tile = j * share // lanes * lanes
+        turn = j * share % lanes
+        g = pltpu.roll(shared_gate[:, tile : tile + lanes], (lanes - turn) % lanes, 1)
+        u = pltpu.roll(shared_up[:, tile : tile + lanes], (lanes + share - turn) % lanes, 1)
+        whole = slice(j * rows, (j + 1) * rows)
+        last = jnp.where(lane < share, g, jnp.where(lane < 2 * share, u, 0.0))
+        last = jnp.where(lane == 2 * share, high[whole], last)
+        last = jnp.where(lane == 2 * share + 1, low[whole], last)
+        last = jnp.where(lane == 2 * share + 2, own_high, last)
+        return jnp.where(lane == 2 * share + 3, own_low, last)
+
     for e in range(experts):
         taken = sorted_rows[e * per * rows : (e + 1) * per * rows].astype(bf16)
         gate, up = dot(taken, gate_ref[e]), dot(taken, up_ref[e])
-        for q in range(per):
+        for q in range(0, per, 2):
             j = e * per + q
-            cut = slice(q * rows, (q + 1) * rows)
-            out_ref[j, :, 0:hidden] = gate[cut].astype(bf16)
-            out_ref[j, :, hidden : 2 * hidden] = up[cut].astype(bf16)
-            tile = j * share // lanes * lanes
-            turn = j * share % lanes
-            g = pltpu.roll(shared_gate[:, tile : tile + lanes], (lanes - turn) % lanes, 1)
-            u = pltpu.roll(shared_up[:, tile : tile + lanes], (lanes + share - turn) % lanes, 1)
-            whole = slice(j * rows, (j + 1) * rows)
-            last = jnp.where(lane < share, g, jnp.where(lane < 2 * share, u, 0.0))
-            last = jnp.where(lane == 2 * share, high[whole], last)
-            last = jnp.where(lane == 2 * share + 1, low[whole], last)
-            last = jnp.where(lane == 2 * share + 2, own_high, last)
-            last = jnp.where(lane == 2 * share + 3, own_low, last)
-            out_ref[j, :, 2 * hidden :] = last.astype(bf16)
+            one, two = slice(q * rows, (q + 1) * rows), slice((q + 1) * rows, (q + 2) * rows)
+            for at, a, b in (
+                (slice(0, hidden), gate[one], gate[two]),
+                (slice(hidden, 2 * hidden), up[one], up[two]),
+                (slice(2 * hidden, 2 * hidden + lanes), last_block(j), last_block(j + 1)),
+            ):
+                keep_ref[j // 2, :, at] = jnp.where(even, a, b).astype(bf16)
+                send_ref[j // 2, :, at] = jnp.where(even, b, a).astype(bf16)
+
+
+def pair(keep_ref, got_ref, out_ref):
+    pairs, rows, width = keep_ref.shape
+    total = keep_ref[...].astype(f32) + got_ref[...].astype(f32)
+    wide = width - lanes
+    out_ref[:, :, :wide] = total[:, :, :wide].astype(bf16)
+    last = total[:, :, wide:]
+    lane = iota(last.shape, 2)
+    share = wide // 2 // (2 * pairs)
+    for at in (2 * share, 2 * share + 2):
+        high, low = two_parts(last[:, :, at : at + 1] + last[:, :, at + 1 : at + 2])
+        last = jnp.where(lane == at, high, jnp.where(lane == at + 1, low, last))
+    out_ref[:, :, wide:] = last.astype(bf16)
 
 
 def activate(got_ref, inner_ref, own_ref, width):
-    chunks, rows, _ = got_ref.shape
+    rows = got_ref.shape[1]
+    chunks = 2 * got_ref.shape[0]
     hidden = inner_ref.shape[1] - lanes
     share = hidden // chunks
     total = jnp.sum(got_ref[...].astype(f32), axis=0)
@@ -294,28 +270,29 @@
     inner_ref[:, hidden:] = jnp.where(lane < share, silu(both) * up, 0.0).astype(bf16)
 
 
-def contract(inner_ref, back_ref, down_ref, out_ref, done_ref):
+def contract(inner_ref, back_ref, down_ref, shared_ref, centred_ref, gain_ref, inv_ref, out_ref, base_ref):
     experts, hidden, _ = down_ref.shape
-    per = inner_ref.shape[0] // experts
-    outs = [
-        dot(inner_ref[e * per : (e + 1) * per, :hidden], down_ref[e]).astype(bf16)
-        for e in range(experts)
-    ]
+    chunks, rows, _ = inner_ref.shape
+    per = chunks // experts
+    share = hidden // chunks
+    outs = []
+    for e in range(experts):
+        inner = jnp.concatenate(
+            [inner_ref[j, :, :hidden].astype(f32) for j in range(e * per, (e + 1) * per)], axis=0
+        )
+        outs.append(dot(inner.astype(bf16), down_ref[e]).astype(bf16))
     out_ref[...] = dot(back_ref[...], jnp.concatenate(outs, axis=0)).astype(bf16)
-    done_ref[...] = jnp.zeros(done_ref.shape, f32)
-
-
-def share_out(inner_ref, down_ref, centred_ref, gain_ref, inv_ref, behind, base_ref):
-    chunks, _, width = inner_ref.shape
-    hidden = width - lanes
-    share = hidden // chunks
     normed = rounded(centred_ref[...] * inv_ref[...] * gain_ref[...])
-    total = res_scale * normed
-    for j in range(chunks):
-        total += dot(
-            inner_ref[j, :, hidden : hidden + share], down_ref[j * share : (j + 1) * share]
-        )
-    base_ref[...] = total
+    lane = iota((rows, lanes), 1)
+    tiles = []
+    for t in range(hidden // lanes):
+        tile = jnp.zeros((rows, lanes), f32)
+        for k in range(lanes // share):
+            piece = inner_ref[t * (lanes // share) + k, :, hidden:].astype(f32)
+            tile = jnp.where(lane // share == k, pltpu.roll(piece, k * share, 1), tile)
+        tiles.append(tile)
+    shared = jnp.concatenate(tiles, axis=1).astype(bf16)
+    base_ref[...] = res_scale * normed + dot(shared, shared_ref[...])
 
 
 def combine(got_ref, high_ref, low_ref, base_ref, resid_ref, stats_ref):
@@ -376,29 +353,24 @@
     gain1, gain2 = norm1_gain.reshape(1, cols), norm2_gain.reshape(1, cols)
 
     held = (
+        route_ids.T,
+        route_weight.T,
         tokens,
-        w_query,
         decay_down.T,
         decay_up,
-        state,
+        decay_bias.reshape(1, -1),
+        w_query,
         w_key,
         w_value,
         w_outgate,
+        head_gain.reshape(1, -1),
+        state,
         w_output,
-        decay_bias.reshape(1, -1),
-        head_gain.reshape(1, -1),
-    )
-    outgoing, done = local_call(
+    )
+    outgoing, send, high, low, perm, back, own = local_call(
         attend,
-        (struct((tp_count, rows + 8, cols), bf16), struct((8, cols), f32)),
-        held,
-        stay=tuple(range(len(held))),
-        scratch=[pltpu.VMEM(a.shape, a.dtype) for a in held] + [pltpu.SemaphoreType.DMA((13,))],
-    )
-    arrived = to_each(outgoing, "tp")
-    send, high, low, perm, back, own = local_call(
-        place,
         (
+            struct((tp_count, rows + 8, cols), bf16),
             struct((slots, lanes), bf16),
             struct((rows, slots), bf16),
             struct((rows, slots), bf16),
@@ -406,8 +378,12 @@
             struct((slots, slots), bf16),
             struct((rows, cols), f32),
         ),
-        (route_ids.T, route_weight.T, tokens, done),
-    )
+        held,
+        stay=tuple(range(len(held))),
+        scratch=[pltpu.VMEM(a.shape, a.dtype) for a in held]
+        + [pltpu.SemaphoreType.DMA((len(held),))],
+    )
+    arrived = to_each(outgoing, "tp")
 
     def named(body):
         def call(*refs):
@@ -422,30 +398,28 @@
         (arrived, own, gain1, send),
     )
     taken = to_each(sent.reshape(ep_count, per_block, cols), "ep").reshape(slots, cols)
-    partials = local_call(
+    block = struct((tp_count // 2, rows, 2 * hidden + lanes), bf16)
+    keep, give = local_call(
         expand,
-        struct((tp_count, rows, 2 * hidden + lanes), bf16),
+        (block, block),
         (taken, perm, exp_gate, exp_up, sh_gate, sh_up, gain1, centred),
     )
-    parts = to_each(partials, "tp")
-
+    other = lax.ppermute(give, "tp", [(i, i ^ 1) for i in range(tp_count)])
+    partials = local_call(pair, block, (keep, other))
+    same_core = [list(range(core, tp_count, 2)) for core in range(2)]
+    parts = lax.all_to_all(partials, "tp", 0, 0, tiled=True, axis_index_groups=same_core)
     inner, inv = local_call(
         named(activate),
         (struct((rows, hidden + lanes), bf16), struct((rows, cols), f32)),
         (parts,),
     )
-    inners = lax.all_gather(inner, "tp", axis=0, tiled=True)
-    result, done = local_call(
+    inners = lax.all_gather(inner, "tp", axis=0)
+    result, base = local_call(
         contract,
-        (struct((slots, cols), bf16), struct((8, cols), f32)),
-        (inners, back, exp_down),
+        (struct((slots, cols), bf16), struct((rows, cols), f32)),
+        (inners, back, exp_down, sh_down, centred, gain1, inv),
     )
     returned = to_each(result.reshape(ep_count, per_block, cols), "ep").reshape(slots, cols)
-    base = local_call(
-        share_out,
-        struct((rows, cols), f32),
-        (inners.reshape(tp_count, rows, -1), sh_down, centred, gain1, inv, done),
-    )
     resid, stats = local_call(
         combine,
         (struct((rows, cols), f32), struct((tp_count, 8, lanes), f32)),

time: 132 us -> 124 us (0.939)
  blocking collectives: 83.8 us -> 111 us
  waiting for transfers between devices: 20.2 us -> 1.4 us
  starting transfers between devices: 18.3 us -> 3.72 us
  Pallas kernels: 8.76 us -> 7.12 us
    all_to_all x2 -> x0, waiting for transfers between devices: 20.2 us -> none  [to_each(): return lax.all_to_all(value, axis, split_axis=0, concat_axis=0, tiled=True)]
    all_to_all x0 -> x1, blocking collectives: none -> 18.6 us  [per_device(): lax.all_to_all(partials, 'tp', 0, 0, tiled=True, axis_index_groups=same_c...]
    all_to_all x2 -> x0, starting transfers between devices: 18.3 us -> none  [to_each(): return lax.all_to_all(value, axis, split_axis=0, concat_axis=0, tiled=True)]
    all_to_all x3 -> x4, blocking collectives: 68 us -> 76.4 us  [to_each(): return lax.all_to_all(value, axis, split_axis=0, concat_axis=0, tiled=True)]
    ppermute x0 -> x1, starting transfers between devices: none -> 3.72 us  [per_device(): other = lax.ppermute(give, 'tp', [(i, i ^ 1) for i in range(tp_count)])]
    pallas_call x9 -> x8, Pallas kernels: 8.76 us -> 7.12 us  [local_call(): pl.pallas_call(body, out_shape=outs, in_specs=[hbm if k in stay else vmem...]
    ppermute x0 -> x1, waiting for transfers between devices: none -> 1.4 us  [per_device(): other = lax.ppermute(give, 'tp', [(i, i ^ 1) for i in range(tp_count)])]
  transfers between devices with their start and end apart: 2 -> 1, of which waited for: 2 -> 1; matrix products, arithmetic and copies ran while one was open for 0% -> 0% of each run, Pallas kernels for 1% -> 0%
where the time goes in v3:
time: 124 us
  blocking collectives  111 us (90%)
  Pallas kernels  7.12 us (6%)
  starting transfers between devices  3.72 us (3%)
  waiting for transfers between devices  1.4 us (1%)
    all_to_all x4, blocking collectives, to_each(): return lax.all_to_all(value, axis, split_axis=0, concat_axis=0, tiled=True)  76.4 us
    all_to_all x1, blocking collectives, per_device(): lax.all_to_all(partials, 'tp', 0, 0, tiled=True, axis_index_groups=same_c...  18.6 us
    all_gather x1, blocking collectives, per_device(): inners = lax.all_gather(inner, 'tp', axis=0)  16.4 us
    pallas_call x8, Pallas kernels, local_call(): pl.pallas_call(body, out_shape=outs, in_specs=[hbm if k in stay else vmem...  7.12 us
    ppermute x1, starting transfers between devices, per_device(): other = lax.ppermute(give, 'tp', [(i, i ^ 1) for i in range(tp_count)])  3.72 us
  transfers between devices with their start and end apart: 1, of which 1 were waited for; matrix products, arithmetic and copies ran while one was open for 0% of the time, Pallas kernels for 0%

profile of v3, /device:TPU:1, one launch (start us, length us, event | category | flops | bytes accessed | tf_op | source)
XLA Modules:
  0.0 123.8 jit_solution(7634233148831220047)
XLA Ops:
  0.0 0.0 copy-start.6
  0.0 0.0 copy-start
  0.0 0.0 copy-start.1
  0.0 0.0 copy-start.3
  0.0 0.0 copy-start.4
  0.0 4.2 %attend.1 = (bf16[16,32,128]{2,1,0:T(8,128)(2,1)S(1)}, bf16[384,128]{1,0:T(8,128)(2,1)S(1)}, bf16[24,384]{1,0:T(8,128)(2,1)S(1)}, bf16[24,384]{1,0:T(8,128)(2,1)...) custom-call(s32[6,24]{1,0:T(8,128)} %bitcast.22, f32[6,24]{1,0:T(8,128)} %bitcast.23, ...), custom_call_target="tpu_custom_call" | custom-call | tf_op jit(solution)/shard_map/attend/pallas_call | solution.py:25
  4.3 0.0 copy-start.2
  4.3 0.0 copy-start.5
  4.3 22.2 %all_to_all.25.refs_0_ = bf16[16,32,128]{2,1,0:T(8,128)(2,1)S(1)} all-to-all(bf16[16,32,128]{2,1,0:T(8,128)(2,1)S(1)} %get-tuple-element.22), channel_id=1, replica_groups=mesh['ep'=48,'tp'=16] {'tp'}, dimensions={0} | all-to-all | bytes 262144 | tf_op jit(solution)/shard_map/all_to_all | solution.py:321
  26.5 0.0 copy-done.6
  26.5 0.2 dispatch.1
  26.7 25.0 %all_to_all.26 = bf16[48,8,128]{2,1,0:T(8,128)(2,1)S(1)} all-to-all(bf16[48,8,128]{2,1,0:T(8,128)(2,1)S(1)} %bitcast.16), channel_id=1, replica_groups=mesh['ep'=48,'tp'=16] {'ep'}, dimensions={0} | all-to-all | bytes 196608 | tf_op jit(solution)/shard_map/all_to_all | solution.py:321
  51.7 0.0 copy-done
  51.7 0.0 copy-done.1
  51.7 0.0 copy-done.3
  51.7 0.0 copy-done.4
  51.7 0.0 copy-start.7
  51.8 0.5 expand.1
  52.3 3.7 %collective-permute-start = (bf16[8,24,1152]{2,1,0:T(8,128)(2,1)S(1)}, bf16[8,24,1152]{2,1,0:T(8,128)(2,1)S(1)}, u32[]{:S(2)}, u32[]{:S(2)}) collective-permute-start(bf16[8,24,1152]{2,1,0:T(8,128)(2,1)S(1)} %get-tuple-element.29), channel_id=1, source_target_pairs={{0,1},{1,0},{2,3},{3,2},{4,5},{5,4},{6,7},{7,6},{8,9},{9,8},{10,11... | collective-permute-start | bytes 1327112 | tf_op jit(solution)/shard_map/ppermute | solution.py:407
  56.0 1.4 %collective-permute-done.got_ref = bf16[8,24,1152]{2,1,0:T(8,128)(2,1)S(1)} collective-permute-done((bf16[8,24,1152]{2,1,0:T(8,128)(2,1)S(1)}, bf16[8,24,1152]{2,1,0:T(8,128)(2,1)S(1)}, u32[]{:S(2)}, u32[]{:S(2)}) %collective-permute-start) | collective-permute-done | bytes 442400 | tf_op jit(solution)/shard_map/ppermute | solution.py:407
  57.4 0.4 pair.1
  57.9 18.6 %all_to_all.27.refs_0_ = bf16[8,24,1152]{2,1,0:T(8,128)(2,1)S(1)} all-to-all(bf16[8,24,1152]{2,1,0:T(8,128)(2,1)S(1)} %pair.1), channel_id=1, replica_groups={{0,2,4,6,8,10,12,14},{1,3,5,7,9,11,13,15},{16,18,20,22,24,26,28,30},{17..., dimensions={0} | all-to-all | bytes 884736 | tf_op jit(solution)/shard_map/all_to_all | solution.py:410
  76.5 0.2 activate.1
  76.7 16.4 %all-gather = bf16[384,640]{1,0:T(8,128)(2,1)S(1)} all-gather(bf16[24,640]{1,0:T(8,128)(2,1)S(1)} %get-tuple-element.30), channel_id=2, replica_groups=mesh['ep'=48,'tp'=16] {'tp'}, dimensions={0}, use_global_device_ids=true | all-gather | bytes 522240 | tf_op jit(solution)/shard_map/all_gather | solution.py:416
  93.0 0.0 copy-done.2
  93.0 0.0 copy-done.5
  93.0 0.5 contract.1
  93.6 15.6 %all_to_all.28 = bf16[48,8,128]{2,1,0:T(8,128)(2,1)S(1)} all-to-all(bf16[48,8,128]{2,1,0:T(8,128)(2,1)S(1)} %bitcast.15), channel_id=1, replica_groups=mesh['ep'=48,'tp'=16] {'ep'}, dimensions={0} | all-to-all | bytes 196608 | tf_op jit(solution)/shard_map/all_to_all | solution.py:321
  109.2 0.2 combine.1
  109.4 13.7 %all_to_all.29.refs_0_ = f32[16,8,128]{2,1,0:T(8,128)S(1)} all-to-all(f32[16,8,128]{2,1,0:T(8,128)S(1)} %get-tuple-element.37), channel_id=1, replica_groups=mesh['ep'=48,'tp'=16] {'tp'}, dimensions={0} | all-to-all | bytes 131072 | tf_op jit(solution)/shard_map/all_to_all | solution.py:321
  123.1 0.0 copy-done.7
  123.1 0.7 finish.1
Async XLA Ops:
  0.0 26.5 %copy-start.6 = (f32[128]{0:T(128)S(1)}, f32[128]{0:T(128)}, u32[]{:S(2)}) copy-start(f32[128]{0:T(128)} %param.32) | copy-start | bytes 1540
  0.0 51.7 %copy-start = (bf16[4,128,512]{2,1,0:T(8,128)(2,1)S(1)}, bf16[4,128,512]{2,1,0:T(8,128)(2,1)}, u32[]{:S(2)}) copy-start(bf16[4,128,512]{2,1,0:T(8,128)(2,1)} %gate_ref.1) | copy-start | bytes 1572868
  0.0 51.7 %copy-start.1 = (bf16[4,128,512]{2,1,0:T(8,128)(2,1)S(1)}, bf16[4,128,512]{2,1,0:T(8,128)(2,1)}, u32[]{:S(2)}) copy-start(bf16[4,128,512]{2,1,0:T(8,128)(2,1)} %up_ref.1) | copy-start | bytes 1572868
  0.0 51.7 %copy-start.3 = (bf16[128,512]{1,0:T(8,128)(2,1)S(1)}, bf16[128,512]{1,0:T(8,128)(2,1)}, u32[]{:S(2)}) copy-start(bf16[128,512]{1,0:T(8,128)(2,1)} %sg_ref.1) | copy-start | bytes 393220
  0.0 51.7 %copy-start.4 = (bf16[128,512]{1,0:T(8,128)(2,1)S(1)}, bf16[128,512]{1,0:T(8,128)(2,1)}, u32[]{:S(2)}) copy-start(bf16[128,512]{1,0:T(8,128)(2,1)} %su_ref.1) | copy-start | bytes 393220
  4.3 88.8 %copy-start.2 = (bf16[4,512,128]{2,1,0:T(8,128)(2,1)S(1)}, bf16[4,512,128]{2,1,0:T(8,128)(2,1)}, u32[]{:S(2)}) copy-start(bf16[4,512,128]{2,1,0:T(8,128)(2,1)} %down_ref.1) | copy-start | bytes 1572868
  4.3 88.8 %copy-start.5 = (bf16[512,128]{1,0:T(8,128)(2,1)S(1)}, bf16[512,128]{1,0:T(8,128)(2,1)}, u32[]{:S(2)}) copy-start(bf16[512,128]{1,0:T(8,128)(2,1)} %shared_ref.1) | copy-start | bytes 393220
  51.7 71.3 %copy-start.7 = (f32[128]{0:T(128)S(1)}, f32[128]{0:T(128)}, u32[]{:S(2)}) copy-start(f32[128]{0:T(128)} %param.41) | copy-start | bytes 1540
  52.3 5.1 %collective-permute-start = (bf16[8,24,1152]{2,1,0:T(8,128)(2,1)S(1)}, bf16[8,24,1152]{2,1,0:T(8,128)(2,1)S(1)}, u32[]{:S(2)}, u32[]{:S(2)}) collective-permute-start(bf16[8,24,1152]{2,1,0:T(8,128)(2,1)S(1)} %get-tuple-element.29), channel_id=1, source_target_pairs={{0,1},{1,0},{2,3},{3,2},{4,5},{5,4},{6,7},{7,6},{8,9},{9,8},{10,11... | collective-permute-start | bytes 1327112 | tf_op jit(solution)/shard_map/ppermute | solution.py:407

commit v4 on v3

--- a/solution.py
+++ b/solution.py
@@ -299,19 +299,25 @@
     got = got_ref[...]
     resid = base_ref[...] + dot(high_ref[...], got) + dot(low_ref[...], got)
     resid_ref[...] = resid
-    sums = as_row(jnp.sum(resid, axis=1, keepdims=True))
-    squares = as_row(jnp.sum(resid * resid, axis=1, keepdims=True))
-    at = iota((8, lanes), 0)
-    tile = jnp.where(at == 0, sums, jnp.where(at == 1, squares, 0.0))
+    column = jnp.sum(resid, axis=1, keepdims=True)
+    squares = jnp.sum(resid * resid, axis=1, keepdims=True)
+    at, lane = iota(resid.shape, 0), iota(resid.shape, 1)
+    half = lanes // 2
+    seen = jnp.where(lane == at, column, jnp.where(lane == at + half, squares, 0.0))
+    row = jnp.sum(seen, axis=0, keepdims=True)
     for j in range(stats_ref.shape[0]):
-        stats_ref[j] = tile
+        stats_ref[j] = row
 
 
 def finish(got_ref, resid_ref, gain_ref, out_ref, width):
-    rows = resid_ref.shape[0]
     total = jnp.sum(got_ref[...], axis=0)
-    mean = as_column(total[0:1], rows) / width
-    spread = as_column(total[1:2], rows) / width - mean * mean
+    at, lane = iota(resid_ref.shape, 0), iota(resid_ref.shape, 1)
+
+    def column(start):
+        return jnp.sum(jnp.where(lane == at + start, total, 0.0), axis=1, keepdims=True)
+
+    mean = column(0) / width
+    spread = column(lanes // 2) / width - mean * mean
     out_ref[...] = (
         (resid_ref[...] - mean) * lax.rsqrt(spread + norm_eps) * gain_ref[...]
     ).astype(bf16)
@@ -422,7 +428,7 @@
     returned = to_each(result.reshape(ep_count, per_block, cols), "ep").reshape(slots, cols)
     resid, stats = local_call(
         combine,
-        (struct((rows, cols), f32), struct((tp_count, 8, lanes), f32)),
+        (struct((rows, cols), f32), struct((tp_count, 1, lanes), f32)),
         (returned, high, low, base),
     )
     all_stats = to_each(stats, "tp")

time: 124 us -> 123 us (level)
  no operation moved by 1% of the time
where the time goes in v4:
time: 123 us
  blocking collectives  111 us (90%)
  Pallas kernels  7.12 us (6%)
  starting transfers between devices  3.72 us (3%)
  waiting for transfers between devices  1.4 us (1%)
    all_to_all x4, blocking collectives, to_each(): return lax.all_to_all(value, axis, split_axis=0, concat_axis=0, tiled=True)  75.7 us
    all_to_all x1, blocking collectives, per_device(): lax.all_to_all(partials, 'tp', 0, 0, tiled=True, axis_index_groups=same_c...  18.6 us
    all_gather x1, blocking collectives, per_device(): inners = lax.all_gather(inner, 'tp', axis=0)  16.4 us
    pallas_call x8, Pallas kernels, local_call(): pl.pallas_call(body, out_shape=outs, in_specs=[hbm if k in stay else vmem...  7.12 us
    ppermute x1, starting transfers between devices, per_device(): other = lax.ppermute(give, 'tp', [(i, i ^ 1) for i in range(tp_count)])  3.72 us
  transfers between devices with their start and end apart: 1, of which 1 were waited for; matrix products, arithmetic and copies ran while one was open for 0% of the time, Pallas kernels for 0%

profile of v4, /device:TPU:1, one launch (start us, length us, event | category | flops | bytes accessed | tf_op | source)
XLA Modules:
  0.0 123.0 jit_solution(14542769312493744196)
XLA Ops:
  0.0 0.0 copy-start.6
  0.0 0.0 copy-start
  0.0 0.0 copy-start.1
  0.0 0.0 copy-start.3
  0.0 0.0 copy-start.4
  0.0 4.2 %attend.1 = (bf16[16,32,128]{2,1,0:T(8,128)(2,1)S(1)}, bf16[384,128]{1,0:T(8,128)(2,1)S(1)}, bf16[24,384]{1,0:T(8,128)(2,1)S(1)}, bf16[24,384]{1,0:T(8,128)(2,1)...) custom-call(s32[6,24]{1,0:T(8,128)} %bitcast.22, f32[6,24]{1,0:T(8,128)} %bitcast.23, ...), custom_call_target="tpu_custom_call" | custom-call | tf_op jit(solution)/shard_map/attend/pallas_call | solution.py:25
  4.3 0.0 copy-start.2
  4.3 0.0 copy-start.5
  4.3 22.2 %all_to_all.25.refs_0_ = bf16[16,32,128]{2,1,0:T(8,128)(2,1)S(1)} all-to-all(bf16[16,32,128]{2,1,0:T(8,128)(2,1)S(1)} %get-tuple-element.22), channel_id=1, replica_groups=mesh['ep'=48,'tp'=16] {'tp'}, dimensions={0} | all-to-all | bytes 262144 | tf_op jit(solution)/shard_map/all_to_all | solution.py:327
  26.5 0.0 copy-done.6
  26.5 0.2 dispatch.1
  26.7 25.0 %all_to_all.26 = bf16[48,8,128]{2,1,0:T(8,128)(2,1)S(1)} all-to-all(bf16[48,8,128]{2,1,0:T(8,128)(2,1)S(1)} %bitcast.16), channel_id=1, replica_groups=mesh['ep'=48,'tp'=16] {'ep'}, dimensions={0} | all-to-all | bytes 196608 | tf_op jit(solution)/shard_map/all_to_all | solution.py:327
  51.7 0.0 copy-done
  51.7 0.0 copy-done.1
  51.7 0.0 copy-done.3
  51.7 0.0 copy-done.4
  51.7 0.0 copy-start.7
  51.8 0.5 expand.1
  52.3 3.7 %collective-permute-start = (bf16[8,24,1152]{2,1,0:T(8,128)(2,1)S(1)}, bf16[8,24,1152]{2,1,0:T(8,128)(2,1)S(1)}, u32[]{:S(2)}, u32[]{:S(2)}) collective-permute-start(bf16[8,24,1152]{2,1,0:T(8,128)(2,1)S(1)} %get-tuple-element.29), channel_id=1, source_target_pairs={{0,1},{1,0},{2,3},{3,2},{4,5},{5,4},{6,7},{7,6},{8,9},{9,8},{10,11... | collective-permute-start | bytes 1327112 | tf_op jit(solution)/shard_map/ppermute | solution.py:413
  56.0 1.4 %collective-permute-done.got_ref = bf16[8,24,1152]{2,1,0:T(8,128)(2,1)S(1)} collective-permute-done((bf16[8,24,1152]{2,1,0:T(8,128)(2,1)S(1)}, bf16[8,24,1152]{2,1,0:T(8,128)(2,1)S(1)}, u32[]{:S(2)}, u32[]{:S(2)}) %collective-permute-start) | collective-permute-done | bytes 442400 | tf_op jit(solution)/shard_map/ppermute | solution.py:413
  57.4 0.4 pair.1
  57.9 18.6 %all_to_all.27.refs_0_ = bf16[8,24,1152]{2,1,0:T(8,128)(2,1)S(1)} all-to-all(bf16[8,24,1152]{2,1,0:T(8,128)(2,1)S(1)} %pair.1), channel_id=1, replica_groups={{0,2,4,6,8,10,12,14},{1,3,5,7,9,11,13,15},{16,18,20,22,24,26,28,30},{17..., dimensions={0} | all-to-all | bytes 884736 | tf_op jit(solution)/shard_map/all_to_all | solution.py:416
  76.5 0.2 activate.1
  76.7 16.4 %all-gather = bf16[384,640]{1,0:T(8,128)(2,1)S(1)} all-gather(bf16[24,640]{1,0:T(8,128)(2,1)S(1)} %get-tuple-element.30), channel_id=2, replica_groups=mesh['ep'=48,'tp'=16] {'tp'}, dimensions={0}, use_global_device_ids=true | all-gather | bytes 522240 | tf_op jit(solution)/shard_map/all_gather | solution.py:422
  93.0 0.0 copy-done.2
  93.0 0.0 copy-done.5
  93.0 0.5 contract.1
  93.6 15.6 %all_to_all.28 = bf16[48,8,128]{2,1,0:T(8,128)(2,1)S(1)} all-to-all(bf16[48,8,128]{2,1,0:T(8,128)(2,1)S(1)} %bitcast.15), channel_id=1, replica_groups=mesh['ep'=48,'tp'=16] {'ep'}, dimensions={0} | all-to-all | bytes 196608 | tf_op jit(solution)/shard_map/all_to_all | solution.py:327
  109.2 0.2 combine.1
  109.4 12.9 %all_to_all.29.refs_0_ = f32[16,1,128]{2,1,0:T(1,128)S(1)} all-to-all(f32[16,1,128]{2,1,0:T(1,128)S(1)} %get-tuple-element.37), channel_id=1, replica_groups=mesh['ep'=48,'tp'=16] {'tp'}, dimensions={0} | all-to-all | bytes 16384 | tf_op jit(solution)/shard_map/all_to_all | solution.py:327
  122.3 0.0 copy-done.7
  122.3 0.7 finish.1
Async XLA Ops:
  0.0 26.5 %copy-start.6 = (f32[128]{0:T(128)S(1)}, f32[128]{0:T(128)}, u32[]{:S(2)}) copy-start(f32[128]{0:T(128)} %param.32) | copy-start | bytes 1540
  0.0 51.7 %copy-start = (bf16[4,128,512]{2,1,0:T(8,128)(2,1)S(1)}, bf16[4,128,512]{2,1,0:T(8,128)(2,1)}, u32[]{:S(2)}) copy-start(bf16[4,128,512]{2,1,0:T(8,128)(2,1)} %gate_ref.1) | copy-start | bytes 1572868
  0.0 51.7 %copy-start.1 = (bf16[4,128,512]{2,1,0:T(8,128)(2,1)S(1)}, bf16[4,128,512]{2,1,0:T(8,128)(2,1)}, u32[]{:S(2)}) copy-start(bf16[4,128,512]{2,1,0:T(8,128)(2,1)} %up_ref.1) | copy-start | bytes 1572868
  0.0 51.7 %copy-start.3 = (bf16[128,512]{1,0:T(8,128)(2,1)S(1)}, bf16[128,512]{1,0:T(8,128)(2,1)}, u32[]{:S(2)}) copy-start(bf16[128,512]{1,0:T(8,128)(2,1)} %sg_ref.1) | copy-start | bytes 393220
  0.0 51.7 %copy-start.4 = (bf16[128,512]{1,0:T(8,128)(2,1)S(1)}, bf16[128,512]{1,0:T(8,128)(2,1)}, u32[]{:S(2)}) copy-start(bf16[128,512]{1,0:T(8,128)(2,1)} %su_ref.1) | copy-start | bytes 393220
  4.3 88.8 %copy-start.2 = (bf16[4,512,128]{2,1,0:T(8,128)(2,1)S(1)}, bf16[4,512,128]{2,1,0:T(8,128)(2,1)}, u32[]{:S(2)}) copy-start(bf16[4,512,128]{2,1,0:T(8,128)(2,1)} %down_ref.1) | copy-start | bytes 1572868
  4.3 88.8 %copy-start.5 = (bf16[512,128]{1,0:T(8,128)(2,1)S(1)}, bf16[512,128]{1,0:T(8,128)(2,1)}, u32[]{:S(2)}) copy-start(bf16[512,128]{1,0:T(8,128)(2,1)} %shared_ref.1) | copy-start | bytes 393220
  51.7 70.6 %copy-start.7 = (f32[128]{0:T(128)S(1)}, f32[128]{0:T(128)}, u32[]{:S(2)}) copy-start(f32[128]{0:T(128)} %param.41) | copy-start | bytes 1540
  52.3 5.1 %collective-permute-start = (bf16[8,24,1152]{2,1,0:T(8,128)(2,1)S(1)}, bf16[8,24,1152]{2,1,0:T(8,128)(2,1)S(1)}, u32[]{:S(2)}, u32[]{:S(2)}) collective-permute-start(bf16[8,24,1152]{2,1,0:T(8,128)(2,1)S(1)} %get-tuple-element.29), channel_id=1, source_target_pairs={{0,1},{1,0},{2,3},{3,2},{4,5},{5,4},{6,7},{7,6},{8,9},{9,8},{10,11... | collective-permute-start | bytes 1327112 | tf_op jit(solution)/shard_map/ppermute | solution.py:413

commit v5 on v4

--- a/solution.py
+++ b/solution.py
@@ -109,9 +109,10 @@
 
 
 def attend(*refs):
-    count = 13
-    far, out_ref, tables, own_ref = refs[:count], refs[count], refs[count + 1 : count + 6], refs[count + 6]
-    near, sems = refs[count + 7 : -1], refs[-1]
+    count, extra = 13, 4
+    far, refs = refs[: count + extra], refs[count + extra :]
+    out_ref, tables, own_ref, refs = refs[0], refs[1:6], refs[6], refs[7:]
+    near, sems = refs[extra:-1] + refs[:extra], refs[-1]
     ids, weights, tok, dd, du, db, wq, wk, wv, wg, hg, state, wo = range(count)
     copies = [pltpu.make_async_copy(a, b, sems.at[k]) for k, (a, b) in enumerate(zip(far, near))]
     for copy in copies:
@@ -168,6 +169,7 @@
         out_ref[j] = jnp.concatenate(
             [partial[:, j * lanes : (j + 1) * lanes], tail], axis=0
         ).astype(bf16)
+    ready(*range(count, count + extra))
 
 
 def dispatch(got_ref, own_ref, gain_ref, send_ref, rows_ref, centred_ref, width):
@@ -234,10 +236,9 @@
 
 def pair(keep_ref, got_ref, out_ref):
     pairs, rows, width = keep_ref.shape
-    total = keep_ref[...].astype(f32) + got_ref[...].astype(f32)
     wide = width - lanes
-    out_ref[:, :, :wide] = total[:, :, :wide].astype(bf16)
-    last = total[:, :, wide:]
+    out_ref[:, :, :wide] = keep_ref[:, :, :wide] + got_ref[:, :, :wide]
+    last = keep_ref[:, :, wide:].astype(f32) + got_ref[:, :, wide:].astype(f32)
     lane = iota(last.shape, 2)
     share = wide // 2 // (2 * pairs)
     for at in (2 * share, 2 * share + 2):
@@ -373,7 +374,8 @@
         state,
         w_output,
     )
-    outgoing, send, high, low, perm, back, own = local_call(
+    later = (exp_gate, exp_up, sh_gate, sh_up)
+    outgoing, send, high, low, perm, back, own, *later = local_call(
         attend,
         (
             struct((tp_count, rows + 8, cols), bf16),
@@ -383,11 +385,12 @@
             struct((slots, slots), bf16),
             struct((slots, slots), bf16),
             struct((rows, cols), f32),
+            *(struct(a.shape, a.dtype) for a in later),
         ),
-        held,
-        stay=tuple(range(len(held))),
+        held + later,
+        stay=tuple(range(len(held + later))),
         scratch=[pltpu.VMEM(a.shape, a.dtype) for a in held]
-        + [pltpu.SemaphoreType.DMA((len(held),))],
+        + [pltpu.SemaphoreType.DMA((len(held + later),))],
     )
     arrived = to_each(outgoing, "tp")
 
@@ -408,7 +411,7 @@
     keep, give = local_call(
         expand,
         (block, block),
-        (taken, perm, exp_gate, exp_up, sh_gate, sh_up, gain1, centred),
+        (taken, perm, *later, gain1, centred),
     )
     other = lax.ppermute(give, "tp", [(i, i ^ 1) for i in range(tp_count)])
     partials = local_call(pair, block, (keep, other))

time: 123 us -> 123 us (level)
  no operation moved by 1% of the time
where the time goes in v5:
time: 123 us
  blocking collectives  111 us (90%)
  Pallas kernels  7.04 us (6%)
  starting transfers between devices  3.72 us (3%)
  waiting for transfers between devices  1.4 us (1%)
    all_to_all x4, blocking collectives, to_each(): return lax.all_to_all(value, axis, split_axis=0, concat_axis=0, tiled=True)  75.7 us
    all_to_all x1, blocking collectives, per_device(): lax.all_to_all(partials, 'tp', 0, 0, tiled=True, axis_index_groups=same_c...  18.6 us
    all_gather x1, blocking collectives, per_device(): inners = lax.all_gather(inner, 'tp', axis=0)  16.4 us
    pallas_call x8, Pallas kernels, local_call(): pl.pallas_call(body, out_shape=outs, in_specs=[hbm if k in stay else vmem...  7.04 us
    ppermute x1, starting transfers between devices, per_device(): other = lax.ppermute(give, 'tp', [(i, i ^ 1) for i in range(tp_count)])  3.72 us
  transfers between devices with their start and end apart: 1, of which 1 were waited for; matrix products, arithmetic and copies ran while one was open for 0% of the time, Pallas kernels for 0%

profile of v5, /device:TPU:1, one launch (start us, length us, event | category | flops | bytes accessed | tf_op | source)
XLA Modules:
  0.0 122.9 jit_solution(16126877632465356804)
XLA Ops:
  0.0 0.0 copy-start.2
  0.0 4.2 %attend.1 = (bf16[16,32,128]{2,1,0:T(8,128)(2,1)S(1)}, bf16[384,128]{1,0:T(8,128)(2,1)S(1)}, bf16[24,384]{1,0:T(8,128)(2,1)S(1)}, bf16[24,384]{1,0:T(8,128)(2,1)...) custom-call(s32[6,24]{1,0:T(8,128)} %bitcast.22, ...), custom_call_target="tpu_custom_call" | custom-call | tf_op jit(solution)/shard_map/attend/pallas_call | solution.py:25
  4.2 0.0 copy-start
  4.2 0.0 copy-start.1
  4.2 22.2 %all_to_all.25.refs_0_ = bf16[16,32,128]{2,1,0:T(8,128)(2,1)S(1)} all-to-all(bf16[16,32,128]{2,1,0:T(8,128)(2,1)S(1)} %get-tuple-element.26), channel_id=1, replica_groups=mesh['ep'=48,'tp'=16] {'tp'}, dimensions={0} | all-to-all | bytes 262144 | tf_op jit(solution)/shard_map/all_to_all | solution.py:328
  26.4 0.0 copy-done.2
  26.4 0.2 dispatch.1
  26.7 25.0 %all_to_all.26 = bf16[48,8,128]{2,1,0:T(8,128)(2,1)S(1)} all-to-all(bf16[48,8,128]{2,1,0:T(8,128)(2,1)S(1)} %bitcast.16), channel_id=1, replica_groups=mesh['ep'=48,'tp'=16] {'ep'}, dimensions={0} | all-to-all | bytes 196608 | tf_op jit(solution)/shard_map/all_to_all | solution.py:328
  51.7 0.0 copy-start.3
  51.7 0.5 expand.1
  52.2 3.7 %collective-permute-start = (bf16[8,24,1152]{2,1,0:T(8,128)(2,1)S(1)}, bf16[8,24,1152]{2,1,0:T(8,128)(2,1)S(1)}, u32[]{:S(2)}, u32[]{:S(2)}) collective-permute-start(bf16[8,24,1152]{2,1,0:T(8,128)(2,1)S(1)} %get-tuple-element.37), channel_id=1, source_target_pairs={{0,1},{1,0},{2,3},{3,2},{4,5},{5,4},{6,7},{7,6},{8,9},{9,8},{10,11... | collective-permute-start | bytes 1327112 | tf_op jit(solution)/shard_map/ppermute | solution.py:416
  56.0 1.4 %collective-permute-done.got_ref = bf16[8,24,1152]{2,1,0:T(8,128)(2,1)S(1)} collective-permute-done((bf16[8,24,1152]{2,1,0:T(8,128)(2,1)S(1)}, bf16[8,24,1152]{2,1,0:T(8,128)(2,1)S(1)}, u32[]{:S(2)}, u32[]{:S(2)}) %collective-permute-start) | collective-permute-done | bytes 442400 | tf_op jit(solution)/shard_map/ppermute | solution.py:416
  57.4 0.4 pair.1
  57.7 18.6 %all_to_all.27.refs_0_ = bf16[8,24,1152]{2,1,0:T(8,128)(2,1)S(1)} all-to-all(bf16[8,24,1152]{2,1,0:T(8,128)(2,1)S(1)} %pair.1), channel_id=1, replica_groups={{0,2,4,6,8,10,12,14},{1,3,5,7,9,11,13,15},{16,18,20,22,24,26,28,30},{17..., dimensions={0} | all-to-all | bytes 884736 | tf_op jit(solution)/shard_map/all_to_all | solution.py:419
  76.3 0.2 activate.1
  76.5 16.4 %all-gather = bf16[384,640]{1,0:T(8,128)(2,1)S(1)} all-gather(bf16[24,640]{1,0:T(8,128)(2,1)S(1)} %get-tuple-element.38), channel_id=2, replica_groups=mesh['ep'=48,'tp'=16] {'tp'}, dimensions={0}, use_global_device_ids=true | all-gather | bytes 522240 | tf_op jit(solution)/shard_map/all_gather | solution.py:425
  92.9 0.0 copy-done
  92.9 0.0 copy-done.1
  92.9 0.5 contract.1
  93.4 15.6 %all_to_all.28 = bf16[48,8,128]{2,1,0:T(8,128)(2,1)S(1)} all-to-all(bf16[48,8,128]{2,1,0:T(8,128)(2,1)S(1)} %bitcast.15), channel_id=1, replica_groups=mesh['ep'=48,'tp'=16] {'ep'}, dimensions={0} | all-to-all | bytes 196608 | tf_op jit(solution)/shard_map/all_to_all | solution.py:328
  109.0 0.2 combine.1
  109.3 12.9 %all_to_all.29.refs_0_ = f32[16,1,128]{2,1,0:T(1,128)S(1)} all-to-all(f32[16,1,128]{2,1,0:T(1,128)S(1)} %get-tuple-element.45), channel_id=1, replica_groups=mesh['ep'=48,'tp'=16] {'tp'}, dimensions={0} | all-to-all | bytes 16384 | tf_op jit(solution)/shard_map/all_to_all | solution.py:328
  122.2 0.0 copy-done.3
  122.2 0.7 finish.1
Async XLA Ops:
  0.0 26.4 %copy-start.2 = (f32[128]{0:T(128)S(1)}, f32[128]{0:T(128)}, u32[]{:S(2)}) copy-start(f32[128]{0:T(128)} %param.32) | copy-start | bytes 1540
  4.2 88.7 %copy-start = (bf16[4,512,128]{2,1,0:T(8,128)(2,1)S(1)}, bf16[4,512,128]{2,1,0:T(8,128)(2,1)}, u32[]{:S(2)}) copy-start(bf16[4,512,128]{2,1,0:T(8,128)(2,1)} %down_ref.1) | copy-start | bytes 1572868
  4.2 88.7 %copy-start.1 = (bf16[512,128]{1,0:T(8,128)(2,1)S(1)}, bf16[512,128]{1,0:T(8,128)(2,1)}, u32[]{:S(2)}) copy-start(bf16[512,128]{1,0:T(8,128)(2,1)} %shared_ref.1) | copy-start | bytes 393220
  51.7 70.5 %copy-start.3 = (f32[128]{0:T(128)S(1)}, f32[128]{0:T(128)}, u32[]{:S(2)}) copy-start(f32[128]{0:T(128)} %param.41) | copy-start | bytes 1540
  52.2 5.1 %collective-permute-start = (bf16[8,24,1152]{2,1,0:T(8,128)(2,1)S(1)}, bf16[8,24,1152]{2,1,0:T(8,128)(2,1)S(1)}, u32[]{:S(2)}, u32[]{:S(2)}) collective-permute-start(bf16[8,24,1152]{2,1,0:T(8,128)(2,1)S(1)} %get-tuple-element.37), channel_id=1, source_target_pairs={{0,1},{1,0},{2,3},{3,2},{4,5},{5,4},{6,7},{7,6},{8,9},{9,8},{10,11... | collective-permute-start | bytes 1327112 | tf_op jit(solution)/shard_map/ppermute | solution.py:416

commit v6 on v5

--- a/solution.py
+++ b/solution.py
@@ -192,32 +192,30 @@
 def expand(
     rows_ref, perm_ref, gate_ref, up_ref, sg_ref, su_ref, gain_ref, centred_ref, keep_ref, send_ref
 ):
-    pairs, rows, _ = keep_ref.shape
+    pairs, _, _ = keep_ref.shape
+    rows = centred_ref.shape[0]
     experts, _, hidden = gate_ref.shape
     chunks = 2 * pairs
     even = lax.rem(lax.axis_index("tp"), 2) == 0
     sorted_rows = dot(perm_ref[...], rows_ref[...])
     scale = sorted_rows / gain_ref[...]
-    high, low = two_parts(jnp.sum(scale * scale, axis=1, keepdims=True))
+    squares = jnp.sum(scale * scale, axis=1, keepdims=True)
     centred = centred_ref[...]
-    own_high, own_low = two_parts(jnp.sum(centred * centred, axis=1, keepdims=True))
+    own_sums = stat_rows(jnp.sum(centred * centred, axis=1, keepdims=True))
     own = (centred * gain_ref[...]).astype(bf16)
     shared_gate, shared_up = dot(own, sg_ref[...]), dot(own, su_ref[...])
-    lane = iota((rows, lanes), 1)
     share = hidden // chunks
     per = chunks // experts
+    tiles = hidden // lanes
 
     def last_block(j):
         tile = j * share // lanes * lanes
         turn = j * share % lanes
         g = pltpu.roll(shared_gate[:, tile : tile + lanes], (lanes - turn) % lanes, 1)
         u = pltpu.roll(shared_up[:, tile : tile + lanes], (lanes + share - turn) % lanes, 1)
-        whole = slice(j * rows, (j + 1) * rows)
-        last = jnp.where(lane < share, g, jnp.where(lane < 2 * share, u, 0.0))
-        last = jnp.where(lane == 2 * share, high[whole], last)
-        last = jnp.where(lane == 2 * share + 1, low[whole], last)
-        last = jnp.where(lane == 2 * share + 2, own_high, last)
-        return jnp.where(lane == 2 * share + 3, own_low, last)
+        both = jnp.where(iota((rows, lanes), 1) < share, g, u)
+        sums = stat_rows(squares[j * rows : (j + 1) * rows])
+        return folded(both, sums, own_sums)
 
     for e in range(experts):
         taken = sorted_rows[e * per * rows : (e + 1) * per * rows].astype(bf16)
@@ -225,61 +223,100 @@
         for q in range(0, per, 2):
             j = e * per + q
             one, two = slice(q * rows, (q + 1) * rows), slice((q + 1) * rows, (q + 2) * rows)
-            for at, a, b in (
-                (slice(0, hidden), gate[one], gate[two]),
-                (slice(hidden, 2 * hidden), up[one], up[two]),
-                (slice(2 * hidden, 2 * hidden + lanes), last_block(j), last_block(j + 1)),
-            ):
-                keep_ref[j // 2, :, at] = jnp.where(even, a, b).astype(bf16)
-                send_ref[j // 2, :, at] = jnp.where(even, b, a).astype(bf16)
+            for k in range(2 * tiles):
+                part = gate if k < tiles else up
+                at = slice(k % tiles * lanes, (k % tiles + 1) * lanes)
+                here = slice(k * rows, (k + 1) * rows)
+                a, b = part[one, at], part[two, at]
+                keep_ref[j // 2, here] = jnp.where(even, a, b).astype(bf16)
+                send_ref[j // 2, here] = jnp.where(even, b, a).astype(bf16)
+            a, b = last_block(j), last_block(j + 1)
+            here = slice(2 * tiles * rows, 2 * tiles * rows + 16)
+            keep_ref[j // 2, here] = jnp.where(even, a, b).astype(bf16)
+            send_ref[j // 2, here] = jnp.where(even, b, a).astype(bf16)
+
+
+def stat_rows(column):
+    shape = (column.shape[0], lanes)
+    seen = jnp.where(iota(shape, 1) == iota(shape, 0) + lanes // 2, column, 0.0)
+    return two_parts(jnp.sum(seen, axis=0, keepdims=True))
+
+
+def folded(both, sums, own_sums):
+    lane, at = iota((8, lanes), 1), iota((8, lanes), 0)
+    upper = lane >= lanes // 2
+    first = jnp.where(upper, pltpu.roll(both[16:24], lanes // 2, 1), both[0:8])
+    stats = jnp.zeros((8, lanes), f32)
+    for k, row in enumerate((*sums, *own_sums)):
+        stats = jnp.where(at == k, row, stats)
+    second = jnp.where(upper, stats, both[8:16])
+    return jnp.concatenate([first, second], axis=0)
 
 
 def pair(keep_ref, got_ref, out_ref):
-    pairs, rows, width = keep_ref.shape
-    wide = width - lanes
-    out_ref[:, :, :wide] = keep_ref[:, :, :wide] + got_ref[:, :, :wide]
-    last = keep_ref[:, :, wide:].astype(f32) + got_ref[:, :, wide:].astype(f32)
-    lane = iota(last.shape, 2)
-    share = wide // 2 // (2 * pairs)
-    for at in (2 * share, 2 * share + 2):
-        high, low = two_parts(last[:, :, at : at + 1] + last[:, :, at + 1 : at + 2])
-        last = jnp.where(lane == at, high, jnp.where(lane == at + 1, low, last))
-    out_ref[:, :, wide:] = last.astype(bf16)
+    wide = keep_ref.shape[1] - 16
+    out_ref[:, :wide] = keep_ref[:, :wide] + got_ref[:, :wide]
+    for p in range(keep_ref.shape[0]):
+        last = keep_ref[p, wide:].astype(f32) + got_ref[p, wide:].astype(f32)
+        at, upper = iota(last.shape, 0), iota(last.shape, 1) >= lanes // 2
+        for k in (8, 10):
+            high, low = two_parts(last[k : k + 1] + last[k + 1 : k + 2])
+            last = jnp.where(
+                upper & (at == k), high, jnp.where(upper & (at == k + 1), low, last)
+            )
+        out_ref[p, wide:] = last.astype(bf16)
 
 
 def activate(got_ref, inner_ref, own_ref, width):
-    rows = got_ref.shape[1]
+    rows = own_ref.shape[0]
     chunks = 2 * got_ref.shape[0]
-    hidden = inner_ref.shape[1] - lanes
-    share = hidden // chunks
+    tiles = (inner_ref.shape[0] - 8) // rows
+    share = tiles * lanes // chunks
     total = jnp.sum(got_ref[...].astype(f32), axis=0)
-    last = total[:, 2 * hidden :]
+    last = total[2 * tiles * rows :]
 
     def inv_std(at):
-        squares = last[:, at : at + 1] + last[:, at + 1 : at + 2]
-        return lax.rsqrt(squares / width + norm_eps)
-
-    inv = inv_std(2 * share)
-    gate = rounded(total[:, :hidden] * inv)
-    up = rounded(total[:, hidden : 2 * hidden] * inv)
-    inner_ref[:, :hidden] = (silu(gate) * up).astype(bf16)
-    inv = inv_std(2 * share + 2)
+        shape = (rows, lanes)
+        row = last[at : at + 1] + last[at + 1 : at + 2]
+        seen = jnp.where(iota(shape, 1) == iota(shape, 0) + lanes // 2, row, 0.0)
+        return lax.rsqrt(jnp.sum(seen, axis=1, keepdims=True) / width + norm_eps)
+
+    inv = inv_std(8)
+    for k in range(tiles):
+        gate = rounded(total[k * rows : (k + 1) * rows] * inv)
+        up = rounded(total[(tiles + k) * rows : (tiles + k + 1) * rows] * inv)
+        inner_ref[k * rows : (k + 1) * rows] = (silu(gate) * up).astype(bf16)
+    inv = inv_std(10)
     own_ref[...] = jnp.broadcast_to(inv, own_ref.shape)
-    both = rounded(last * inv)
-    up = pltpu.roll(both, lanes - share, 1)
-    lane = iota((rows, lanes), 1)
-    inner_ref[:, hidden:] = jnp.where(lane < share, silu(both) * up, 0.0).astype(bf16)
+    both = jnp.concatenate([last, pltpu.roll(last[0:8], lanes // 2, 1)], axis=0)
+    both = rounded(both * inv)
+    inner = silu(both) * pltpu.roll(both, lanes - share, 1)
+    lane = iota((8, lanes), 1)
+    packed = jnp.zeros((8, lanes), f32)
+    for k in range(rows // 8):
+        moved = pltpu.roll(inner[8 * k : 8 * k + 8], k * share, 1)
+        packed = jnp.where(lane // share == k, moved, packed)
+    inner_ref[tiles * rows :] = packed.astype(bf16)
 
 
 def contract(inner_ref, back_ref, down_ref, shared_ref, centred_ref, gain_ref, inv_ref, out_ref, base_ref):
     experts, hidden, _ = down_ref.shape
-    chunks, rows, _ = inner_ref.shape
+    chunks = inner_ref.shape[0]
+    rows = centred_ref.shape[0]
     per = chunks // experts
+    width = hidden // lanes
     share = hidden // chunks
     outs = []
     for e in range(experts):
         inner = jnp.concatenate(
-            [inner_ref[j, :, :hidden].astype(f32) for j in range(e * per, (e + 1) * per)], axis=0
+            [
+                jnp.concatenate(
+                    [inner_ref[j, k * rows : (k + 1) * rows].astype(f32) for k in range(width)],
+                    axis=1,
+                )
+                for j in range(e * per, (e + 1) * per)
+            ],
+            axis=0,
         )
         outs.append(dot(inner.astype(bf16), down_ref[e]).astype(bf16))
     out_ref[...] = dot(back_ref[...], jnp.concatenate(outs, axis=0)).astype(bf16)
@@ -289,8 +326,11 @@
     for t in range(hidden // lanes):
         tile = jnp.zeros((rows, lanes), f32)
         for k in range(lanes // share):
-            piece = inner_ref[t * (lanes // share) + k, :, hidden:].astype(f32)
-            tile = jnp.where(lane // share == k, pltpu.roll(piece, k * share, 1), tile)
+            piece = inner_ref[t * (lanes // share) + k, width * rows :].astype(f32)
+            turned = [
+                pltpu.roll(piece, (k - b) * share % lanes, 1) for b in range(rows // 8)
+            ]
+            tile = jnp.where(lane // share == k, jnp.concatenate(turned, axis=0), tile)
         tiles.append(tile)
     shared = jnp.concatenate(tiles, axis=1).astype(bf16)
     base_ref[...] = res_scale * normed + dot(shared, shared_ref[...])
@@ -407,7 +447,8 @@
         (arrived, own, gain1, send),
     )
     taken = to_each(sent.reshape(ep_count, per_block, cols), "ep").reshape(slots, cols)
-    block = struct((tp_count // 2, rows, 2 * hidden + lanes), bf16)
+    tiles = hidden // lanes
+    block = struct((tp_count // 2, 2 * tiles * rows + 16, lanes), bf16)
     keep, give = local_call(
         expand,
         (block, block),
@@ -419,7 +460,7 @@
     parts = lax.all_to_all(partials, "tp", 0, 0, tiled=True, axis_index_groups=same_core)
     inner, inv = local_call(
         named(activate),
-        (struct((rows, hidden + lanes), bf16), struct((rows, cols), f32)),
+        (struct((tiles * rows + 8, lanes), bf16), struct((rows, cols), f32)),
         (parts,),
     )
     inners = lax.all_gather(inner, "tp", axis=0)

time: 123 us -> 122 us (level)
  no operation moved by 1% of the time
where the time goes in v6:
time: 122 us
  blocking collectives  110 us (90%)
  Pallas kernels  6.82 us (6%)
  starting transfers between devices  3.72 us (3%)
  waiting for transfers between devices  1.37 us (1%)
    all_to_all x4, blocking collectives, to_each(): return lax.all_to_all(value, axis, split_axis=0, concat_axis=0, tiled=True)  75.7 us
    all_to_all x1, blocking collectives, per_device(): lax.all_to_all(partials, 'tp', 0, 0, tiled=True, axis_index_groups=same_c...  18.2 us
    all_gather x1, blocking collectives, per_device(): inners = lax.all_gather(inner, 'tp', axis=0)  16.2 us
    pallas_call x8, Pallas kernels, local_call(): pl.pallas_call(body, out_shape=outs, in_specs=[hbm if k in stay else vmem...  6.82 us
    ppermute x1, starting transfers between devices, per_device(): other = lax.ppermute(give, 'tp', [(i, i ^ 1) for i in range(tp_count)])  3.72 us
  transfers between devices with their start and end apart: 1, of which 1 were waited for; matrix products, arithmetic and copies ran while one was open for 0% of the time, Pallas kernels for 0%

profile of v6, /device:TPU:1, one launch (start us, length us, event | category | flops | bytes accessed | tf_op | source)
XLA Modules:
  0.0 122.2 jit_solution(1706598283255745893)
XLA Ops:
  0.0 0.0 copy-start.2
  0.0 4.2 %attend.1 = (bf16[16,32,128]{2,1,0:T(8,128)(2,1)S(1)}, bf16[384,128]{1,0:T(8,128)(2,1)S(1)}, bf16[24,384]{1,0:T(8,128)(2,1)S(1)}, bf16[24,384]{1,0:T(8,128)(2,1)...) custom-call(s32[6,24]{1,0:T(8,128)} %bitcast.22, ...), custom_call_target="tpu_custom_call" | custom-call | tf_op jit(solution)/shard_map/attend/pallas_call | solution.py:25
  4.2 0.0 copy-start
  4.2 0.0 copy-start.1
  4.2 22.2 %all_to_all.25.refs_0_ = bf16[16,32,128]{2,1,0:T(8,128)(2,1)S(1)} all-to-all(bf16[16,32,128]{2,1,0:T(8,128)(2,1)S(1)} %get-tuple-element.26), channel_id=1, replica_groups=mesh['ep'=48,'tp'=16] {'tp'}, dimensions={0} | all-to-all | bytes 262144 | tf_op jit(solution)/shard_map/all_to_all | solution.py:368
  26.4 0.0 copy-done.2
  26.4 0.2 dispatch.1
  26.7 25.0 %all_to_all.26 = bf16[48,8,128]{2,1,0:T(8,128)(2,1)S(1)} all-to-all(bf16[48,8,128]{2,1,0:T(8,128)(2,1)S(1)} %bitcast.16), channel_id=1, replica_groups=mesh['ep'=48,'tp'=16] {'ep'}, dimensions={0} | all-to-all | bytes 196608 | tf_op jit(solution)/shard_map/all_to_all | solution.py:368
  51.7 0.0 copy-start.3
  51.7 0.6 expand.1
  52.3 3.7 %collective-permute-start = (bf16[8,208,128]{2,1,0:T(8,128)(2,1)S(1)}, bf16[8,208,128]{2,1,0:T(8,128)(2,1)S(1)}, u32[]{:S(2)}, u32[]{:S(2)}) collective-permute-start(bf16[8,208,128]{2,1,0:T(8,128)(2,1)S(1)} %get-tuple-element.37), channel_id=1, source_target_pairs={{0,1},{1,0},{2,3},{3,2},{4,5},{5,4},{6,7},{7,6},{8,9},{9,8},{10,11... | collective-permute-start | bytes 1277960 | tf_op jit(solution)/shard_map/ppermute | solution.py:457
  56.0 1.4 %collective-permute-done.got_ref = bf16[8,208,128]{2,1,0:T(8,128)(2,1)S(1)} collective-permute-done((bf16[8,208,128]{2,1,0:T(8,128)(2,1)S(1)}, bf16[8,208,128]{2,1,0:T(8,128)(2,1)S(1)}, u32[]{:S(2)}, u32[]{:S(2)}) %collective-permute-start) | collective-permute-done | bytes 426016 | tf_op jit(solution)/shard_map/ppermute | solution.py:457
  57.4 0.1 pair.1
  57.5 18.2 %all_to_all.27.refs_0_ = bf16[8,208,128]{2,1,0:T(8,128)(2,1)S(1)} all-to-all(bf16[8,208,128]{2,1,0:T(8,128)(2,1)S(1)} %pair.1), channel_id=1, replica_groups={{0,2,4,6,8,10,12,14},{1,3,5,7,9,11,13,15},{16,18,20,22,24,26,28,30},{17..., dimensions={0} | all-to-all | bytes 851968 | tf_op jit(solution)/shard_map/all_to_all | solution.py:460
  75.7 0.2 activate.1
  76.0 16.2 %all-gather = bf16[1664,128]{1,0:T(8,128)(2,1)S(1)} all-gather(bf16[104,128]{1,0:T(8,128)(2,1)S(1)} %get-tuple-element.38), channel_id=2, replica_groups=mesh['ep'=48,'tp'=16] {'tp'}, dimensions={0}, use_global_device_ids=true | all-gather | bytes 452608 | tf_op jit(solution)/shard_map/all_gather | solution.py:466
  92.2 0.0 copy-done
  92.2 0.0 copy-done.1
  92.2 0.5 contract.1
  92.7 15.6 %all_to_all.28 = bf16[48,8,128]{2,1,0:T(8,128)(2,1)S(1)} all-to-all(bf16[48,8,128]{2,1,0:T(8,128)(2,1)S(1)} %bitcast.15), channel_id=1, replica_groups=mesh['ep'=48,'tp'=16] {'ep'}, dimensions={0} | all-to-all | bytes 196608 | tf_op jit(solution)/shard_map/all_to_all | solution.py:368
  108.3 0.2 combine.1
  108.5 13.0 %all_to_all.29.refs_0_ = f32[16,1,128]{2,1,0:T(1,128)S(1)} all-to-all(f32[16,1,128]{2,1,0:T(1,128)S(1)} %get-tuple-element.45), channel_id=1, replica_groups=mesh['ep'=48,'tp'=16] {'tp'}, dimensions={0} | all-to-all | bytes 16384 | tf_op jit(solution)/shard_map/all_to_all | solution.py:368
  121.5 0.0 copy-done.3
  121.5 0.7 finish.1
Async XLA Ops:
  0.0 26.4 %copy-start.2 = (f32[128]{0:T(128)S(1)}, f32[128]{0:T(128)}, u32[]{:S(2)}) copy-start(f32[128]{0:T(128)} %param.32) | copy-start | bytes 1540
  4.2 87.9 %copy-start = (bf16[4,512,128]{2,1,0:T(8,128)(2,1)S(1)}, bf16[4,512,128]{2,1,0:T(8,128)(2,1)}, u32[]{:S(2)}) copy-start(bf16[4,512,128]{2,1,0:T(8,128)(2,1)} %down_ref.1) | copy-start | bytes 1572868
  4.2 87.9 %copy-start.1 = (bf16[512,128]{1,0:T(8,128)(2,1)S(1)}, bf16[512,128]{1,0:T(8,128)(2,1)}, u32[]{:S(2)}) copy-start(bf16[512,128]{1,0:T(8,128)(2,1)} %shared_ref.1) | copy-start | bytes 393220
  51.7 69.8 %copy-start.3 = (f32[128]{0:T(128)S(1)}, f32[128]{0:T(128)}, u32[]{:S(2)}) copy-start(f32[128]{0:T(128)} %param.41) | copy-start | bytes 1540
  52.3 5.1 %collective-permute-start = (bf16[8,208,128]{2,1,0:T(8,128)(2,1)S(1)}, bf16[8,208,128]{2,1,0:T(8,128)(2,1)S(1)}, u32[]{:S(2)}, u32[]{:S(2)}) collective-permute-start(bf16[8,208,128]{2,1,0:T(8,128)(2,1)S(1)} %get-tuple-element.37), channel_id=1, source_target_pairs={{0,1},{1,0},{2,3},{3,2},{4,5},{5,4},{6,7},{7,6},{8,9},{9,8},{10,11... | collective-permute-start | bytes 1277960 | tf_op jit(solution)/shard_map/ppermute | solution.py:457

commit v7 on v6

--- a/solution.py
+++ b/solution.py
@@ -114,9 +114,19 @@
     out_ref, tables, own_ref, refs = refs[0], refs[1:6], refs[6], refs[7:]
     near, sems = refs[extra:-1] + refs[:extra], refs[-1]
     ids, weights, tok, dd, du, db, wq, wk, wv, wg, hg, state, wo = range(count)
-    copies = [pltpu.make_async_copy(a, b, sems.at[k]) for k, (a, b) in enumerate(zip(far, near))]
-    for copy in copies:
-        copy.start()
+    copies = {
+        k: pltpu.make_async_copy(a, b, sems.at[k])
+        for k, (a, b) in enumerate(zip(far, near))
+        if k != wo
+    }
+    half = near[wo].shape[1] // 2
+    halves = [
+        pltpu.make_async_copy(far[wo].at[:, cut], near[wo].at[:, cut], sems.at[at])
+        for cut, at in ((pl.ds(0, half), wo), (pl.ds(half, half), count + extra))
+    ]
+    for k in range(count + extra):
+        for copy in halves if k == wo else (copies[k],):
+            copy.start()
 
     def ready(*which):
         for k in which:
@@ -157,8 +167,11 @@
     attended = carried + jnp.sum(queries * keys, axis=1, keepdims=True) * values
     inv_norm = lax.rsqrt(jnp.mean(attended * attended, axis=1, keepdims=True) + norm_eps)
     head_out = (attended * inv_norm * near[hg][...] * silu(gate)).astype(bf16)
-    ready(wo)
-    partial = rounded(dot(head_out, near[wo][...]))
+    partials = []
+    for k, copy in enumerate(halves):
+        copy.wait()
+        partials.append(rounded(dot(head_out, near[wo][:, k * half : (k + 1) * half])))
+    partial = jnp.concatenate(partials, axis=1)
     row = as_row(jnp.sum(partial, axis=1, keepdims=True))
     high = rounded(row)
     middle = rounded(row - high)
@@ -430,7 +443,7 @@
         held + later,
         stay=tuple(range(len(held + later))),
         scratch=[pltpu.VMEM(a.shape, a.dtype) for a in held]
-        + [pltpu.SemaphoreType.DMA((len(held + later),))],
+        + [pltpu.SemaphoreType.DMA((len(held + later) + 1,))],
     )
     arrived = to_each(outgoing, "tp")
 

time: 122 us -> 123 us (level)
  no operation moved by 1% of the time
where the time goes in v7:
time: 123 us; the launch traced here: 122 us
  blocking collectives  110 us (89%)
  Pallas kernels  6.94 us (6%)
  starting transfers between devices  3.72 us (3%)
  waiting for transfers between devices  1.37 us (1%)
    all_to_all x4, blocking collectives, to_each(): return lax.all_to_all(value, axis, split_axis=0, concat_axis=0, tiled=True)  75.7 us
    all_to_all x1, blocking collectives, per_device(): lax.all_to_all(partials, 'tp', 0, 0, tiled=True, axis_index_groups=same_c...  18.2 us
    all_gather x1, blocking collectives, per_device(): inners = lax.all_gather(inner, 'tp', axis=0)  16.2 us
    pallas_call x8, Pallas kernels, local_call(): pl.pallas_call(body, out_shape=outs, in_specs=[hbm if k in stay else vmem...  6.94 us
    ppermute x1, starting transfers between devices, per_device(): other = lax.ppermute(give, 'tp', [(i, i ^ 1) for i in range(tp_count)])  3.72 us
  transfers between devices with their start and end apart: 1, of which 1 were waited for; matrix products, arithmetic and copies ran while one was open for 0% of the time, Pallas kernels for 0%

profile of v7, /device:TPU:1, one launch (start us, length us, event | category | flops | bytes accessed | tf_op | source)
XLA Modules:
  0.0 122.3 jit_solution(17426112790034185454)
XLA Ops:
  0.0 0.0 copy-start.2
  0.0 4.3 %attend.1 = (bf16[16,32,128]{2,1,0:T(8,128)(2,1)S(1)}, bf16[384,128]{1,0:T(8,128)(2,1)S(1)}, bf16[24,384]{1,0:T(8,128)(2,1)S(1)}, bf16[24,384]{1,0:T(8,128)(2,1)...) custom-call(s32[6,24]{1,0:T(8,128)} %bitcast.22, ...), custom_call_target="tpu_custom_call" | custom-call | tf_op jit(solution)/shard_map/attend/pallas_call | solution.py:25
  4.3 0.0 copy-start
  4.4 0.0 copy-start.1
  4.4 22.2 %all_to_all.25.refs_0_ = bf16[16,32,128]{2,1,0:T(8,128)(2,1)S(1)} all-to-all(bf16[16,32,128]{2,1,0:T(8,128)(2,1)S(1)} %get-tuple-element.26), channel_id=1, replica_groups=mesh['ep'=48,'tp'=16] {'tp'}, dimensions={0} | all-to-all | bytes 262144 | tf_op jit(solution)/shard_map/all_to_all | solution.py:381
  26.6 0.0 copy-done.2
  26.6 0.2 dispatch.1
  26.8 25.0 %all_to_all.26 = bf16[48,8,128]{2,1,0:T(8,128)(2,1)S(1)} all-to-all(bf16[48,8,128]{2,1,0:T(8,128)(2,1)S(1)} %bitcast.16), channel_id=1, replica_groups=mesh['ep'=48,'tp'=16] {'ep'}, dimensions={0} | all-to-all | bytes 196608 | tf_op jit(solution)/shard_map/all_to_all | solution.py:381
  51.8 0.0 copy-start.3
  51.8 0.6 expand.1
  52.4 3.7 %collective-permute-start = (bf16[8,208,128]{2,1,0:T(8,128)(2,1)S(1)}, bf16[8,208,128]{2,1,0:T(8,128)(2,1)S(1)}, u32[]{:S(2)}, u32[]{:S(2)}) collective-permute-start(bf16[8,208,128]{2,1,0:T(8,128)(2,1)S(1)} %get-tuple-element.37), channel_id=1, source_target_pairs={{0,1},{1,0},{2,3},{3,2},{4,5},{5,4},{6,7},{7,6},{8,9},{9,8},{10,11... | collective-permute-start | bytes 1277960 | tf_op jit(solution)/shard_map/ppermute | solution.py:470
  56.1 1.4 %collective-permute-done.got_ref = bf16[8,208,128]{2,1,0:T(8,128)(2,1)S(1)} collective-permute-done((bf16[8,208,128]{2,1,0:T(8,128)(2,1)S(1)}, bf16[8,208,128]{2,1,0:T(8,128)(2,1)S(1)}, u32[]{:S(2)}, u32[]{:S(2)}) %collective-permute-start) | collective-permute-done | bytes 426016 | tf_op jit(solution)/shard_map/ppermute | solution.py:470
  57.5 0.1 pair.1
  57.6 18.2 %all_to_all.27.refs_0_ = bf16[8,208,128]{2,1,0:T(8,128)(2,1)S(1)} all-to-all(bf16[8,208,128]{2,1,0:T(8,128)(2,1)S(1)} %pair.1), channel_id=1, replica_groups={{0,2,4,6,8,10,12,14},{1,3,5,7,9,11,13,15},{16,18,20,22,24,26,28,30},{17..., dimensions={0} | all-to-all | bytes 851968 | tf_op jit(solution)/shard_map/all_to_all | solution.py:473
  75.8 0.2 activate.1
  76.1 16.2 %all-gather = bf16[1664,128]{1,0:T(8,128)(2,1)S(1)} all-gather(bf16[104,128]{1,0:T(8,128)(2,1)S(1)} %get-tuple-element.38), channel_id=2, replica_groups=mesh['ep'=48,'tp'=16] {'tp'}, dimensions={0}, use_global_device_ids=true | all-gather | bytes 452608 | tf_op jit(solution)/shard_map/all_gather | solution.py:479
  92.3 0.0 copy-done
  92.3 0.0 copy-done.1
  92.3 0.5 contract.1
  92.8 15.6 %all_to_all.28 = bf16[48,8,128]{2,1,0:T(8,128)(2,1)S(1)} all-to-all(bf16[48,8,128]{2,1,0:T(8,128)(2,1)S(1)} %bitcast.15), channel_id=1, replica_groups=mesh['ep'=48,'tp'=16] {'ep'}, dimensions={0} | all-to-all | bytes 196608 | tf_op jit(solution)/shard_map/all_to_all | solution.py:381
  108.4 0.2 combine.1
  108.6 13.0 %all_to_all.29.refs_0_ = f32[16,1,128]{2,1,0:T(1,128)S(1)} all-to-all(f32[16,1,128]{2,1,0:T(1,128)S(1)} %get-tuple-element.45), channel_id=1, replica_groups=mesh['ep'=48,'tp'=16] {'tp'}, dimensions={0} | all-to-all | bytes 16384 | tf_op jit(solution)/shard_map/all_to_all | solution.py:381
  121.6 0.0 copy-done.3
  121.6 0.7 finish.1
Async XLA Ops:
  0.0 26.6 %copy-start.2 = (f32[128]{0:T(128)S(1)}, f32[128]{0:T(128)}, u32[]{:S(2)}) copy-start(f32[128]{0:T(128)} %param.32) | copy-start | bytes 1540
  4.3 87.9 %copy-start = (bf16[4,512,128]{2,1,0:T(8,128)(2,1)S(1)}, bf16[4,512,128]{2,1,0:T(8,128)(2,1)}, u32[]{:S(2)}) copy-start(bf16[4,512,128]{2,1,0:T(8,128)(2,1)} %down_ref.1) | copy-start | bytes 1572868
  4.4 87.9 %copy-start.1 = (bf16[512,128]{1,0:T(8,128)(2,1)S(1)}, bf16[512,128]{1,0:T(8,128)(2,1)}, u32[]{:S(2)}) copy-start(bf16[512,128]{1,0:T(8,128)(2,1)} %shared_ref.1) | copy-start | bytes 393220
  51.8 69.8 %copy-start.3 = (f32[128]{0:T(128)S(1)}, f32[128]{0:T(128)}, u32[]{:S(2)}) copy-start(f32[128]{0:T(128)} %param.41) | copy-start | bytes 1540
  52.4 5.1 %collective-permute-start = (bf16[8,208,128]{2,1,0:T(8,128)(2,1)S(1)}, bf16[8,208,128]{2,1,0:T(8,128)(2,1)S(1)}, u32[]{:S(2)}, u32[]{:S(2)}) collective-permute-start(bf16[8,208,128]{2,1,0:T(8,128)(2,1)S(1)} %get-tuple-element.37), channel_id=1, source_target_pairs={{0,1},{1,0},{2,3},{3,2},{4,5},{5,4},{6,7},{7,6},{8,9},{9,8},{10,11... | collective-permute-start | bytes 1277960 | tf_op jit(solution)/shard_map/ppermute | solution.py:470
